TPU v7x, 32 devices: a whole 2x2x4 slice. The times are simulated.
32 devices in a mesh: sp: 8 (over z, x), tp: 4 (over y, core).
Axes of the slice: x: 2, y: 2, z: 4, core: 2. Of those that a mesh axis runs over, the one named last changes fastest.
Arguments:
- queries: bfloat16 [8192, 1024], P('sp', 'tp'), may hold values from -75 to 75
- key_rows: bfloat16 [8192, 1024], P('sp', 'tp'), may hold values from -4 to 4
- value_rows: bfloat16 [8192, 1024], P('sp', 'tp'), may hold values from -6 to 6
- cum_gate: float32 [16, 8192], P('tp'), may hold values from -1172 to 0, as said below
- residual: bfloat16 [8192, 2048], P(('sp', 'tp')), may hold values from -6 to 6
- out_weight: bfloat16 [1024, 2048], replicated, may hold values from -0.1875 to 0.1875
- gain_mix: float32 [2048], replicated, may hold values from 0.1 to 1.9
- gain_pre: float32 [2048], replicated, may hold values from 0.1 to 1.9
- gain_post: float32 [2048], replicated, may hold values from 0.1 to 1.9
- route_ids: int32 [8192, 2], P(('sp', 'tp')), may hold values from 0 to 31, all different within a row; in each aligned block of 256 rows (0 to 255, 256 to 511, ...) at most 22 rows name the same one
- route_weight: float32 [8192, 2], P(('sp', 'tp')), may hold values from 0.2 to 1
- w_gate: bfloat16 [32, 2048, 512], P(('sp', 'tp')), may hold values from -0.125 to 0.125
- w_up: bfloat16 [32, 2048, 512], P(('sp', 'tp')), may hold values from -0.125 to 0.125
- w_down: bfloat16 [32, 512, 2048], P(('sp', 'tp')), may hold values from -0.25 to 0.25
Outputs:
- layer_out: bfloat16 [8192, 2048], P(('sp', 'tp'))
Inputs may be any that keep to these rules, and one draw needn't show every extreme that they name: `route_ids`: each row names 2 different experts; in the rows of one device no expert is named more than 22 times, a bound that some block reaches. `cum_gate`: along the positions each head's values never rise.
All inputs are finite; a program needn't handle non-finite values.
Results may differ from a plain program's by a relative error of at most 0.018.
Values may be sent and summed in bfloat16 or wider, within the bound.
A program may use at most 128 MiB of HBM per device.

v0:
```python
import functools
import math

import jax
import jax.numpy as jnp
from jax import lax
from jax.experimental import pallas as pl
from jax.experimental.pallas import tpu as pltpu
from jax.sharding import PartitionSpec as P

HEAD_DIM = 64
NORM_EPS = 1e-06
MASKED = -1e30


def rms_scale(rows, gain):
    mean_sq = jnp.mean(rows * rows, axis=-1, keepdims=True)
    return rows * lax.rsqrt(mean_sq + NORM_EPS) * gain


def bf16_parts(values):
    parts = []
    for _ in range(3):
        part = lax.reduce_precision(values, 8, 7)
        parts.append(part.astype(jnp.bfloat16))
        values = values - part
    return parts


def pack_kernel(q_ref, k_ref, v_ref, one_ref, two_ref, *, shares, n_tp):
    tok_dev, width = q_ref.shape
    first = tok_dev - two_ref.shape[1]
    rows_dev = tok_dev // n_tp
    sub = rows_dev // shares
    for h in range(width // HEAD_DIM):
        cols = pl.ds(h * HEAD_DIM, HEAD_DIM)
        pairs = jnp.concatenate((k_ref[:, cols], v_ref[:, cols]), axis=1)
        for r in range(shares):
            dest = h * shares + r
            one_ref[dest, :first] = pairs[:first]
            two_ref[dest] = pairs[first:]
            for t in range(n_tp // 2):
                low, high = (
                    q_ref[pl.ds((t + step) * rows_dev + r * sub, sub), cols]
                    for step in (0, n_tp // 2)
                )
                one_ref[dest, pl.ds(first + t * sub, sub)] = jnp.concatenate((low, high), axis=1)


def pack(queries, key_rows, value_rows, first, shares, n_tp):
    tok_dev, width = queries.shape
    dests = width // HEAD_DIM * shares
    half = tok_dev // shares // 2
    shapes = [(dests, first + half, 2 * HEAD_DIM), (dests, tok_dev - first, 2 * HEAD_DIM)]
    return pl.pallas_call(
        functools.partial(pack_kernel, shares=shares, n_tp=n_tp),
        out_shape=[jax.ShapeDtypeStruct(shape, jnp.bfloat16) for shape in shapes],
        in_specs=[pl.BlockSpec(memory_space=pltpu.VMEM)] * 3,
        out_specs=[pl.BlockSpec(memory_space=pltpu.VMEM)] * 2,
        compiler_params=pltpu.CompilerParams(vmem_limit_bytes=32 * 2**20),
        name="pack",
    )(queries, key_rows, value_rows)


def assemble_kernel(in_ref, out_ref, *, shares, n_tp, local_heads):
    half = in_ref.shape[1]
    for t in range(n_tp):
        for h in range(0, local_heads, 2):
            for r in range(shares):
                left = in_ref[(h * shares + r) * n_tp + t]
                right = in_ref[((h + 1) * shares + r) * n_tp + t]
                for part in range(2):
                    cols = slice(part * HEAD_DIM, (part + 1) * HEAD_DIM)
                    out_ref[
                        pl.ds((2 * r + part) * half, half),
                        pl.ds((t * local_heads + h) * HEAD_DIM, 2 * HEAD_DIM),
                    ] = jnp.concatenate((left[:, cols], right[:, cols]), axis=1)


def assemble(heads, shares, n_tp, local_heads):
    shape = (2 * shares * heads.shape[1], n_tp * local_heads * HEAD_DIM)
    return pl.pallas_call(
        functools.partial(
            assemble_kernel, shares=shares, n_tp=n_tp, local_heads=local_heads
        ),
        out_shape=jax.ShapeDtypeStruct(shape, jnp.bfloat16),
        in_specs=[pl.BlockSpec(memory_space=pltpu.VMEM)],
        out_specs=pl.BlockSpec(memory_space=pltpu.VMEM),
        name="assemble",
    )(heads)


def flash_kernel(*refs, begun, span, shares, sub, rows_dev, n_tp):
    if begun:
        q_ref, kv_ref, side_q_ref, side_k_ref, state_ref, o_ref, k_aug, v_aug = refs
    else:
        q_ref, kv_ref, side_q_ref, side_k_ref, o_ref, k_aug, v_aug = refs
    lo, hi = span
    count = hi - lo
    tile = pl.program_id(0)
    rank = lax.rem(lax.axis_index("sp"), shares)

    @pl.when(tile == 0)
    def _():
        lane = lax.broadcasted_iota(jnp.int32, (count, 2 * HEAD_DIM), 1)

        def one(src, carry):
            kv = kv_ref[src, :count].astype(jnp.float32)
            side = side_k_ref[src, lo:hi].astype(jnp.float32)
            k_aug[src] = jnp.where(lane < HEAD_DIM, kv, side).astype(jnp.bfloat16)
            ones = (lane == 0).astype(jnp.float32)
            v_aug[src] = jnp.where(lane < HEAD_DIM, ones, kv).astype(jnp.bfloat16)
            return carry

        lax.fori_loop(0, kv_ref.shape[0], one, 0)

    packed = q_ref[0]
    queries = jnp.concatenate((packed[:, :HEAD_DIM], packed[:, HEAD_DIM:]), axis=0)
    queries = queries * jnp.bfloat16(HEAD_DIM**-0.5)
    queries = jnp.concatenate((queries, side_q_ref[:, HEAD_DIM:]), axis=1)
    rows = queries.shape[0]
    out_lane = lax.broadcasted_iota(jnp.int32, (rows, 2 * HEAD_DIM), 1)

    def step(src, state, masked):
        peak, acc = state
        scores = lax.dot_general(
            queries, k_aug[src], (((1,), (1,)), ((), ())), preferred_element_type=jnp.float32
        )
        if masked:
            row = lax.broadcasted_iota(jnp.int32, (rows, 1), 0)
            pos = row // sub * rows_dev + rank * sub + row % sub
            key = lo + lax.broadcasted_iota(jnp.int32, (1, count), 1)
            scores = jnp.where(key <= pos, scores, MASKED)
        new_peak = jnp.maximum(peak, jnp.max(scores, axis=1, keepdims=True))
        probs = jnp.exp(scores - new_peak).astype(jnp.bfloat16)
        acc = acc * jnp.exp(peak - new_peak) + jnp.dot(
            probs, v_aug[src], preferred_element_type=jnp.float32
        )
        return new_peak, acc

    if begun:
        before = state_ref[...]
        kept = jnp.max(jnp.where(out_lane == 1, before, -jnp.inf), axis=1, keepdims=True)
        state = (kept, jnp.where(out_lane == 1, 0.0, before))
    else:
        state = (
            jnp.full((rows, 1), MASKED, jnp.float32),
            jnp.zeros((rows, 2 * HEAD_DIM), jnp.float32),
        )
    state = lax.fori_loop(0, tile, lambda i, state: step(i, state, False), state)
    peak, acc = step(tile, state, True)
    if not begun:
        o_ref[...] = jnp.where(out_lane == 1, peak, acc)
        return
    out = acc[:, HEAD_DIM:] / acc[:, :1]
    half = sub // 2
    for t in range(n_tp):
        top, low = (out[t * sub + step : t * sub + step + half] for step in (0, half))
        o_ref[t] = jnp.concatenate((top, low), axis=1).astype(o_ref.dtype)


def flash(got, kv, side_q, side_k, state, span, first, sub, rows_dev, n_tp, shares):
    n_sp, count = kv.shape[0], span[1] - span[0]
    chunk = n_tp * sub
    lanes = 2 * HEAD_DIM
    whole = pl.BlockSpec(memory_space=pltpu.VMEM)
    begun = state is not None
    wide = pl.BlockSpec((chunk, lanes), lambda i: (i, 0))
    if begun:
        out_shape = jax.ShapeDtypeStruct((n_sp * n_tp, sub // 2, lanes), jnp.bfloat16)
        out_spec = pl.BlockSpec((n_tp, sub // 2, lanes), lambda i: (i, 0, 0))
    else:
        out_shape = jax.ShapeDtypeStruct((n_sp * chunk, lanes), jnp.float32)
        out_spec = wide
    first_q = first // (chunk // 2)
    body = functools.partial(
        flash_kernel,
        begun=begun,
        span=span,
        shares=shares,
        sub=sub,
        rows_dev=rows_dev,
        n_tp=n_tp,
    )
    q_spec = pl.BlockSpec((1, chunk // 2, lanes), lambda i: (i, first_q, 0))
    pairs = n_sp * (n_sp + 1) // 2 * chunk * count
    return pl.pallas_call(
        body,
        grid=(n_sp,),
        out_shape=out_shape,
        in_specs=[q_spec, whole, wide, whole] + [wide] * begun,
        out_specs=out_spec,
        scratch_shapes=[pltpu.VMEM((n_sp, count, lanes), jnp.bfloat16)] * 2,
        compiler_params=pltpu.CompilerParams(vmem_limit_bytes=50 * 2**20),
        cost_estimate=pl.CostEstimate(
            flops=8 * lanes * pairs, bytes_accessed=2**22, transcendentals=pairs
        ),
        name="flash",
    )(got, kv, side_q, side_k, *([state] if begun else []))


def local(
    queries,
    key_rows,
    value_rows,
    cum_gate,
    residual,
    out_weight,
    gain_mix,
    gain_pre,
    gain_post,
    route_ids,
    route_weight,
    w_gate,
    w_up,
    w_down,
):
    tok_dev, feature_width = queries.shape
    local_heads = feature_width // HEAD_DIM
    n_sp, n_tp = lax.axis_size("sp"), lax.axis_size("tp")
    shares = n_sp // local_heads
    rows_dev = residual.shape[0]
    sub = rows_dev // shares
    chunk = n_tp * sub
    half = chunk // 2
    first = tok_dev * 5 // 8 // half * half
    one, two = pack(queries, key_rows, value_rows, first, shares, n_tp)
    got = lax.all_to_all(one, "sp", split_axis=0, concat_axis=0, tiled=True)
    got, two = lax.optimization_barrier((got, two))
    got_two = lax.all_to_all(two, "sp", split_axis=0, concat_axis=0, tiled=True)

    me = lax.axis_index("sp")
    gate = lax.dynamic_index_in_dim(cum_gate, me // shares, 0, keepdims=False)
    gate_q = gate.reshape(n_sp * n_tp, shares, sub)
    gate_q = lax.dynamic_index_in_dim(gate_q, me % shares, 1, keepdims=False).reshape(-1)
    ones_q = jnp.ones((n_sp * chunk,), jnp.bfloat16)
    ones_k = jnp.ones((n_sp * tok_dev,), jnp.bfloat16)
    lanes = jnp.arange(2 * HEAD_DIM)
    place_side = (lanes == HEAD_DIM + jnp.arange(6)[:, None]).astype(jnp.bfloat16)

    def side_lanes(parts):
        return lax.dot_general(
            jnp.stack(parts), place_side, (((0,), (0,)), ((), ())), preferred_element_type=jnp.float32
        ).astype(jnp.bfloat16)

    side_q = side_lanes(bf16_parts(gate_q) + [ones_q] * 3)
    side_k = side_lanes([ones_k] * 3 + bf16_parts(-gate))
    side_k = side_k.reshape(n_sp, tok_dev, 2 * HEAD_DIM)
    fixed = (first, sub, rows_dev, n_tp, shares)
    state = flash(got, got, side_q, side_k, None, (0, first), *fixed)
    out = flash(got, got_two, side_q, side_k, state, (first, tok_dev), *fixed)
    heads = lax.all_to_all(out, ("sp", "tp"), split_axis=0, concat_axis=0, tiled=True)
    head_rows = assemble(heads, shares, n_tp, local_heads)
    projected = jnp.dot(head_rows, out_weight, preferred_element_type=jnp.float32)
    stream = (residual.astype(jnp.float32) + rms_scale(projected, gain_mix)).astype(jnp.bfloat16)
    stream_wide = lax.optimization_barrier(stream).astype(jnp.float32)
    normed = rms_scale(stream_wide, gain_pre).astype(jnp.bfloat16)
    top_count = route_ids.shape[1]
    experts_all = n_sp * n_tp
    capacity = max(2, (4 * rows_dev * top_count + 3 * experts_all - 1) // (3 * experts_all))
    capacity = (capacity + 7) // 8 * 8
    flat_ids = route_ids.reshape(-1)
    item = lax.iota(jnp.int32, rows_dev * top_count)
    earlier = (item[None, :] < item[:, None]) & (flat_ids[None, :] == flat_ids[:, None])
    slot_index = flat_ids * capacity + jnp.sum(earlier.astype(jnp.int32), axis=1)
    slot_index = slot_index.reshape(rows_dev, top_count)
    slots_all = experts_all * capacity
    slot = lax.iota(jnp.int32, slots_all)
    place = sum((slot_index[:, k, None] == slot).astype(jnp.bfloat16) for k in range(top_count))
    outgoing = lax.dot_general(
        place, normed, (((0,), (0,)), ((), ())), preferred_element_type=jnp.float32
    ).astype(jnp.bfloat16)
    outgoing = outgoing.reshape(experts_all, capacity, -1)
    arrived = lax.all_to_all(outgoing, ("sp", "tp"), split_axis=0, concat_axis=0, tiled=True)
    flat_rows = arrived.reshape(slots_all, -1)
    gate_act = jnp.dot(flat_rows, w_gate[0], preferred_element_type=jnp.float32)
    up_act = jnp.dot(flat_rows, w_up[0], preferred_element_type=jnp.float32)
    hidden = (jax.nn.silu(gate_act) * up_act).astype(jnp.bfloat16)
    expert_out = jnp.dot(hidden, w_down[0], preferred_element_type=jnp.float32).astype(jnp.bfloat16)
    returned = lax.all_to_all(
        expert_out.reshape(experts_all, capacity, -1),
        ("sp", "tp"),
        split_axis=0,
        concat_axis=0,
        tiled=True,
    ).reshape(slots_all, -1)
    weigh = sum(
        jnp.where(slot_index[:, k, None] == slot, route_weight[:, k, None], 0.0)
        for k in range(top_count)
    )
    combined = sum(
        jnp.dot(part, returned, preferred_element_type=jnp.float32) for part in bf16_parts(weigh)
    )
    return (stream_wide + rms_scale(combined, gain_post)).astype(jnp.bfloat16)


def solution(mesh):
    return jax.shard_map(
        local,
        mesh=mesh,
        in_specs=(
            P("sp", "tp"),
            P("sp", "tp"),
            P("sp", "tp"),
            P("tp", None),
            P(("sp", "tp"), None),
            P(),
            P(),
            P(),
            P(),
            P(("sp", "tp"), None),
            P(("sp", "tp"), None),
            P(("sp", "tp"), None, None),
            P(("sp", "tp"), None, None),
            P(("sp", "tp"), None, None),
        ),
        out_specs=P(("sp", "tp"), None),
        check_vma=False,
    )
```

profile of v0, /device:TPU:27, one launch (start us, length us, event | category | flops | bytes accessed | tf_op | source)
XLA Modules:
  0.0 312.3 jit_solution(4033443789800401812)
XLA Ops:
  0.0 1.2 copy-done.4
  3.3 1.4 pack.1
  5.9 5.4 %all-to-all-start = ((bf16[8,768,128]{2,1,0:T(8,128)(2,1)}), bf16[8,768,128]{2,1,0:T(8,128)(2,1)}, u32[]{:S(2)}, u32[]{:S(2)}) async-start(bf16[8,768,128]{2,1,0:T(8,128)(2,1)} %copy-done.1), calls=%async_computation | async-start | bytes 3145728 | tf_op jit(solution)/shard_map/all_to_all | solution.py:228
  12.3 34.5 %all-to-all-done.refs_0_.refs_1_ = bf16[8,768,128]{2,1,0:T(8,128)(2,1)} async-done(((bf16[8,768,128]{2,1,0:T(8,128)(2,1)}), bf16[8,768,128]{2,1,0:T(8,128)(2,1)}, u32[]{:S(2)}, u32[]{:S(2)}) %all-to-all-start) | async-done | bytes 1572896 | tf_op jit(solution)/shard_map/all_to_all | solution.py:228
  46.8 5.4 %all-to-all-start.1 = ((bf16[8,512,128]{2,1,0:T(8,128)(2,1)}), bf16[8,512,128]{2,1,0:T(8,128)(2,1)S(1)}, u32[]{:S(2)}, u32[]{:S(2)}) async-start(bf16[8,512,128]{2,1,0:T(8,128)(2,1)} %get-tuple-element.12), calls=%async_computation.1 | async-start | bytes 2097152 | tf_op jit(solution)/shard_map/all_to_all | solution.py:230
  53.3 2.3 convolution_convert_fusion
  55.6 26.4 %flash.2.refs_4_ = f32[4096,128]{1,0:T(8,128)} custom-call(bf16[8,768,128]{2,1,0:T(8,128)(2,1)} %all-to-all-done.refs_0_.refs_1_, bf16[8,768,128]{2,1,0:T(8,128)(2,1)} %all-to-all-done.refs_0_.refs_1_, bf16[4096,128]{1,0:T(8,128)(2,1)S(1)} %convolution_convert_fusion.1.refs_2_, bf16[8,1024,128]{2,1,0:T(8,128)(2,1)} %bitcast.43), custom_call_target="tpu_custom_call" | custom-call | flops 9663676416 | bytes 4194304 | tf_op jit(solution)/shard_map/flash/pallas_call | solution.py:187
  82.0 1.2 copy-done.3
  83.2 27.3 %flash.3 = bf16[32,64,128]{2,1,0:T(8,128)(2,1)S(1)} custom-call(bf16[8,768,128]{2,1,0:T(8,128)(2,1)} %all-to-all-done.refs_0_.refs_1_, bf16[8,512,128]{2,1,0:T(8,128)(2,1)S(1)} %all-to-all-done.1.refs_1_, bf16[4096,128]{1,0:T(8,128)(2,1)S(1)} %copy-done.3, bf16[8,1024,128]{2,1,0:T(8,128)(2,1)} %bitcast.44, f32[4096,128]{1,0:T(8,128)} %flash.2.refs_4_), custom_call_target="tpu_custom_call" | custom-call | flops 9663676416 | bytes 4194304 | tf_op jit(solution)/shard_map/flash/pallas_call | solution.py:187
  111.3 6.5 %all-to-all-start.2 = ((bf16[32,64,128]{2,1,0:T(8,128)(2,1)}), bf16[32,64,128]{2,1,0:T(8,128)(2,1)S(1)}, u32[]{:S(2)}, u32[]{:S(2)}) async-start(bf16[32,64,128]{2,1,0:T(8,128)(2,1)} %copy-done.7), calls=%async_computation.2 | async-start | bytes 1048576 | tf_op jit(solution)/shard_map/all_to_all | solution.py:252
  118.7 11.8 %all-to-all-done.2.in_ref = bf16[32,64,128]{2,1,0:T(8,128)(2,1)S(1)} async-done(((bf16[32,64,128]{2,1,0:T(8,128)(2,1)}), bf16[32,64,128]{2,1,0:T(8,128)(2,1)S(1)}, u32[]{:S(2)}, u32[]{:S(2)}) %all-to-all-start.2) | async-done | bytes 524320 | tf_op jit(solution)/shard_map/all_to_all | solution.py:252
  131.2 2.1 assemble.1
  133.3 3.8 %multiply_reduce_fusion.1 = (f32[256]{0:T(256)S(1)}, f32[256,2048]{1,0:T(8,128)S(1)}) fusion(bf16[256,1024]{1,0:T(8,128)(2,1)} %assemble.1, bf16[1024,2048]{1,0:T(8,128)(2,1)} %param.19), kind=kOutput, calls=%fused_computation.20 | convolution fusion | flops 1074790144 | bytes 6816768 | tf_op jit(solution)/shard_map/dot_general | solution.py:254
  137.8 1.2 convolution_convert_fusion.3
  139.1 74.7 %all_to_all.25 = bf16[32,24,2048]{2,1,0:T(8,128)(2,1)S(1)} all-to-all(bf16[32,24,2048]{2,1,0:T(8,128)(2,1)S(1)} %bitcast.42), channel_id=1, replica_groups=mesh['sp'=8,'tp'=4] {'sp','tp'}, dimensions={0} | all-to-all | bytes 6291456 | tf_op jit(solution)/shard_map/all_to_all | solution.py:274
  213.8 1.7 copy-done.8
  215.5 3.0 fusion.7
  218.4 8.1 %convolution_convert_fusion.2 = bf16[768,2048]{1,0:T(8,128)(2,1)} fusion(bf16[1,512,2048]{2,1,0:T(8,128)(2,1)S(1)} %copy-done, f32[768,512]{1,0:T(8,128)} %fusion.7, bf16[768,2048]{1,0:T(8,128)(2,1)} %bitcast.41, bf16[1,2048,512]{2,1,0:T(8,128)(2,1)} %param.26), kind=kOutput, calls=%fused_computation.2 | convolution fusion | flops 3225157632 | bytes 12058624 | tf_op jit(solution)/shard_map/dot_general | solution.py:279
  226.6 6.0 %all-to-all-start.4 = ((bf16[32,24,2048]{2,1,0:T(8,128)(2,1)}), bf16[32,24,2048]{2,1,0:T(8,128)(2,1)}, u32[]{:S(2)}, u32[]{:S(2)}) async-start(bf16[32,24,2048]{2,1,0:T(8,128)(2,1)} %bitcast.39), calls=%async_computation.4 | async-start | bytes 6291456 | tf_op jit(solution)/shard_map/all_to_all | solution.py:280
  232.5 68.9 %all-to-all-done.4 = bf16[32,24,2048]{2,1,0:T(8,128)(2,1)} async-done(((bf16[32,24,2048]{2,1,0:T(8,128)(2,1)}), bf16[32,24,2048]{2,1,0:T(8,128)(2,1)}, u32[]{:S(2)}, u32[]{:S(2)}) %all-to-all-start.4) | async-done | bytes 3145760 | tf_op jit(solution)/shard_map/all_to_all | solution.py:280
  301.5 3.0 fusion.22
  304.5 3.1 convolution_add_fusion.1
  307.7 3.2 %multiply_reduce_fusion = (f32[256]{0:T(256)S(1)}, f32[256,2048]{1,0:T(8,128)S(1)}) fusion(f32[256,2048]{1,0:T(8,128)S(1)} %convolution_add_fusion.1, bf16[768,2048]{1,0:T(8,128)(2,1)} %bitcast.13, f32[256]{0:T(256)S(1)} %bitcast.59, s32[256]{0:T(256)S(1)} %bitcast.53, f32[256]{0:T(256)S(1)} %bitcast.56, s32[256]{0:T(256)S(1)} %bitcast.49), kind=kOutput, calls=%fused_computation.18 | convolution fusion | flops 809041664 | bytes 7345152 | tf_op jit(solution)/shard_map/dot_general | solution.py:292
  310.9 1.4 fusion.3
  (56 shorter events, 8.4 us)
Async XLA Ops:
  0.0 218.4 %copy-start = (bf16[1,512,2048]{2,1,0:T(8,128)(2,1)S(1)}, bf16[1,512,2048]{2,1,0:T(8,128)(2,1)}, u32[]{:S(2)}) copy-start(bf16[1,512,2048]{2,1,0:T(8,128)(2,1)} %param.27) | copy-start | bytes 6291460
  0.0 1.2 copy-start.4
  1.2 1.0 copy-start.5
  2.2 1.0 copy-start.6
  4.7 1.2 copy-start.1
  5.9 40.9 %all-to-all-start = ((bf16[8,768,128]{2,1,0:T(8,128)(2,1)}), bf16[8,768,128]{2,1,0:T(8,128)(2,1)}, u32[]{:S(2)}, u32[]{:S(2)}) async-start(bf16[8,768,128]{2,1,0:T(8,128)(2,1)} %copy-done.1), calls=%async_computation | async-start | bytes 3145728 | tf_op jit(solution)/shard_map/all_to_all | solution.py:228
  46.8 35.2 %all-to-all-start.1 = ((bf16[8,512,128]{2,1,0:T(8,128)(2,1)}), bf16[8,512,128]{2,1,0:T(8,128)(2,1)S(1)}, u32[]{:S(2)}, u32[]{:S(2)}) async-start(bf16[8,512,128]{2,1,0:T(8,128)(2,1)} %get-tuple-element.12), calls=%async_computation.1 | async-start | bytes 2097152 | tf_op jit(solution)/shard_map/all_to_all | solution.py:230
  53.3 2.3 copy-start.2
  82.0 1.2 copy-start.3
  83.2 34.6 %copy-start.13 = (s32[256,2]{0,1:T(2,128)S(1)}, s32[256,2]{0,1:T(2,128)}, u32[]{:S(2)}) copy-start(s32[256,2]{0,1:T(2,128)} %param.23) | copy-start | bytes 6148
  110.5 0.8 copy-start.7
  111.3 19.1 %all-to-all-start.2 = ((bf16[32,64,128]{2,1,0:T(8,128)(2,1)}), bf16[32,64,128]{2,1,0:T(8,128)(2,1)S(1)}, u32[]{:S(2)}, u32[]{:S(2)}) async-start(bf16[32,64,128]{2,1,0:T(8,128)(2,1)} %copy-done.7), calls=%async_computation.2 | async-start | bytes 1048576 | tf_op jit(solution)/shard_map/all_to_all | solution.py:252
  130.5 0.8 copy-start.9
  133.3 3.8 %copy-start.10 = (bf16[256,2048]{1,0:T(8,128)(2,1)S(1)}, bf16[256,2048]{1,0:T(8,128)(2,1)}, u32[]{:S(2)}) copy-start(bf16[256,2048]{1,0:T(8,128)(2,1)} %param.18) | copy-start | bytes 3145732
  133.3 3.8 %copy-start.11 = (f32[2048]{0:T(1024)S(1)}, f32[2048]{0:T(1024)}, u32[]{:S(2)}) copy-start(f32[2048]{0:T(1024)} %param.20) | copy-start | bytes 24580
  137.1 0.7 copy-start.16
  139.1 76.4 %copy-start.15 = (bf16[1,2048,512]{2,1,0:T(8,128)(2,1)S(1)}, bf16[1,2048,512]{2,1,0:T(8,128)(2,1)}, u32[]{:S(2)}) copy-start(bf16[1,2048,512]{2,1,0:T(8,128)(2,1)} %param.25) | copy-start | bytes 6291460
  213.8 1.7 copy-start.8
  226.6 6.0 %copy-start.14 = (f32[256,2]{0,1:T(2,128)S(1)}, f32[256,2]{0,1:T(2,128)}, u32[]{:S(2)}) copy-start(f32[256,2]{0,1:T(2,128)} %param.24) | copy-start | bytes 6148
  226.6 74.9 %all-to-all-start.4 = ((bf16[32,24,2048]{2,1,0:T(8,128)(2,1)}), bf16[32,24,2048]{2,1,0:T(8,128)(2,1)}, u32[]{:S(2)}, u32[]{:S(2)}) async-start(bf16[32,24,2048]{2,1,0:T(8,128)(2,1)} %bitcast.39), calls=%async_computation.4 | async-start | bytes 6291456 | tf_op jit(solution)/shard_map/all_to_all | solution.py:280
  307.7 3.3 %copy-start.12 = (f32[2048]{0:T(1024)S(1)}, f32[2048]{0:T(1024)}, u32[]{:S(2)}) copy-start(f32[2048]{0:T(1024)} %param.22) | copy-start | bytes 24580
where the time goes:
time: 317 us; the launch traced here: 312 us
  waiting for transfers between devices  115 us (36%)
  blocking collectives  74.7 us (24%)
  Pallas kernels  57.2 us (18%)
  matrix products  28.3 us (9%)
  starting transfers between devices  23.4 us (7%)
  local copies, waits for them, and re-layouts  9.91 us (3%)
  other arithmetic  3.4 us (1%)
    all_to_all x1, blocking collectives, local(): lax.all_to_all(outgoing, ('sp', 'tp'), split_axis=0, concat_axis=0, tiled...  74.7 us
    all_to_all x1, waiting for transfers between devices, local(): lax.all_to_all(expert_out.reshape(experts_all, capacity, -1), ('sp', 'tp'...  68.9 us
    pallas_call x2, Pallas kernels, flash(): pl.pallas_call(body, grid=(n_sp,), out_shape=out_shape, in_specs=[q_spec,...  53.7 us
    all_to_all x1, waiting for transfers between devices, local(): got = lax.all_to_all(one, 'sp', split_axis=0, concat_axis=0, tiled=True)  34.5 us
    all_to_all x1, waiting for transfers between devices, local(): lax.all_to_all(out, ('sp', 'tp'), split_axis=0, concat_axis=0, tiled=True)  11.8 us
    dot_general x3, matrix products, local(): jnp.dot(part, returned, preferred_element_type=jnp.float32)  9.39 us
    unnamed x35, local copies, waits for them, and re-layouts  9.11 us
    dot_general x1, matrix products, local(): jnp.dot(hidden, w_down[0], preferred_element_type=jnp.float32)  8.13 us
  transfers between devices with their start and end apart: 4, of which 3 were waited for; matrix products, arithmetic and copies ran while one was open for 2% of the time, Pallas kernels for 8%

commit v1 on v0

--- a/solution.py
+++ b/solution.py
@@ -11,6 +11,9 @@
 HEAD_DIM = 64
 NORM_EPS = 1e-06
 MASKED = -1e30
+MESH = pl.DeviceIdType.MESH
+CHUNKS = 4
+GROUPS = 4
 
 
 def rms_scale(rows, gain):
@@ -199,6 +202,161 @@
     )(got, kv, side_q, side_k, *([state] if begun else []))
 
 
+def expert_kernel(
+    out_ref, wg_hbm, wu_hbm, wd_hbm, weigh_ref, stream_ref, gain_ref, o_ref,
+    arrived, made, returned, wg, wu, wd, gate_acc, up_acc, hidden, comb,
+    w_sem, own_sem, send_sem, recv_sem, *, n_tp, chunks,
+):
+    n, cap, width = out_ref.shape
+    part = width // chunks
+    sp, tp = lax.axis_index("sp"), lax.axis_index("tp")
+    me = sp * n_tp + tp
+
+    def peer(o):
+        d = lax.rem(me + o, n)
+        return d, (d // n_tp, lax.rem(d, n_tp))
+
+    loads = [
+        pltpu.make_async_copy(src, dst, w_sem.at[i])
+        for i, (src, dst) in enumerate(((wg_hbm, wg), (wu_hbm, wu), (wd_hbm, wd)))
+    ]
+    for load in loads:
+        load.start()
+
+    barrier = pltpu.get_barrier_semaphore()
+
+    def greet(o, carry):
+        pl.semaphore_signal(barrier, inc=1, device_id=peer(o)[1], device_id_type=MESH)
+        return carry
+
+    lax.fori_loop(1, n, greet, 0)
+    pl.semaphore_wait(barrier, n - 1)
+
+    def cols(c):
+        return pl.ds(c * part, part)
+
+    def send_all(src, dst, c, slot):
+        def one(o, carry):
+            d, where = peer(o)
+            pltpu.make_async_remote_copy(
+                src_ref=src.at[d, :, cols(c)],
+                dst_ref=dst.at[me, :, cols(c)],
+                send_sem=send_sem.at[slot],
+                recv_sem=recv_sem.at[slot],
+                device_id=where,
+                device_id_type=MESH,
+            ).start()
+            return carry
+
+        pltpu.make_async_copy(src.at[me, :, cols(c)], dst.at[me, :, cols(c)], own_sem.at[slot]).start()
+        lax.fori_loop(1, n, one, 0)
+
+    def all_copies(src, dst, c, slot):
+        return pltpu.make_async_remote_copy(
+            src_ref=src.at[pl.ds(0, n - 1), :, cols(c)],
+            dst_ref=dst.at[pl.ds(0, n - 1), :, cols(c)],
+            send_sem=send_sem.at[slot],
+            recv_sem=recv_sem.at[slot],
+            device_id=peer(1)[1],
+            device_id_type=MESH,
+        )
+
+    def wait_all(src, dst, c, slot):
+        pltpu.make_async_copy(src.at[me, :, cols(c)], dst.at[me, :, cols(c)], own_sem.at[slot]).wait()
+        all_copies(src, dst, c, slot).wait_recv()
+
+    for c in range(chunks):
+        send_all(out_ref, arrived, c, c)
+    for load in loads[:2]:
+        load.wait()
+    group = n // GROUPS
+    rows = group * cap
+
+    for c in range(chunks):
+        wait_all(out_ref, arrived, c, c)
+
+        def gate_up(g, carry, c=c):
+            x = arrived[pl.ds(g * group, group), :, cols(c)].reshape(rows, part)
+            at = pl.ds(pl.multiple_of(g * rows, rows), rows)
+            gate = jnp.dot(x, wg[cols(c), :], preferred_element_type=jnp.float32)
+            up = jnp.dot(x, wu[cols(c), :], preferred_element_type=jnp.float32)
+            if c > 0:
+                gate, up = gate + gate_acc[at, :], up + up_acc[at, :]
+            if c < chunks - 1:
+                gate_acc[at, :] = gate
+                up_acc[at, :] = up
+            else:
+                hidden[at, :] = (jax.nn.silu(gate) * up).astype(jnp.bfloat16)
+            return carry
+
+        lax.fori_loop(0, GROUPS, gate_up, 0)
+    loads[2].wait()
+    for c in range(chunks):
+
+        def down(g, carry, c=c):
+            at = pl.ds(pl.multiple_of(g * rows, rows), rows)
+            y = jnp.dot(hidden[at, :], wd[:, cols(c)], preferred_element_type=jnp.float32)
+            made[pl.ds(g * group, group), :, cols(c)] = y.astype(jnp.bfloat16).reshape(group, cap, part)
+            return carry
+
+        lax.fori_loop(0, GROUPS, down, 0)
+        send_all(made, returned, c, chunks + c)
+    total = jnp.zeros((o_ref.shape[0], 1), jnp.float32)
+    for c in range(chunks):
+        wait_all(made, returned, c, chunks + c)
+        back = returned[:, :, cols(c)].reshape(n * cap, part)
+        mixed = sum(
+            jnp.dot(weigh_ref[i], back, preferred_element_type=jnp.float32)
+            for i in range(weigh_ref.shape[0])
+        )
+        comb[:, cols(c)] = mixed
+        total = total + jnp.sum(mixed * mixed, axis=1, keepdims=True)
+    scale = lax.rsqrt(total / width + NORM_EPS)
+    for c in range(chunks):
+        o_ref[:, cols(c)] = (
+            stream_ref[:, cols(c)].astype(jnp.float32) + comb[:, cols(c)] * scale * gain_ref[:, cols(c)]
+        ).astype(jnp.bfloat16)
+    for c in range(chunks):
+        all_copies(out_ref, arrived, c, c).wait_send()
+        all_copies(made, returned, c, chunks + c).wait_send()
+
+
+def experts(outgoing, w_gate, w_up, w_down, weigh, stream, gain, n_tp):
+    n, cap, width = outgoing.shape
+    hidden = w_gate.shape[1]
+    slots = n * cap
+    chunks = CHUNKS
+    vmem = pl.BlockSpec(memory_space=pltpu.VMEM)
+    hbm = pl.BlockSpec(memory_space=pl.ANY)
+    bf16, f32 = jnp.bfloat16, jnp.float32
+    return pl.pallas_call(
+        functools.partial(expert_kernel, n_tp=n_tp, chunks=chunks),
+        out_shape=jax.ShapeDtypeStruct(stream.shape, bf16),
+        in_specs=[vmem, hbm, hbm, hbm, vmem, vmem, vmem],
+        out_specs=vmem,
+        scratch_shapes=[
+            pltpu.VMEM((n, cap, width), bf16),
+            pltpu.VMEM((n, cap, width), bf16),
+            pltpu.VMEM((n, cap, width), bf16),
+            pltpu.VMEM(w_gate.shape, bf16),
+            pltpu.VMEM(w_up.shape, bf16),
+            pltpu.VMEM(w_down.shape, bf16),
+            pltpu.VMEM((slots, hidden), f32),
+            pltpu.VMEM((slots, hidden), f32),
+            pltpu.VMEM((slots, hidden), bf16),
+            pltpu.VMEM(stream.shape, f32),
+            pltpu.SemaphoreType.DMA((3,)),
+            pltpu.SemaphoreType.DMA((2 * chunks,)),
+            pltpu.SemaphoreType.DMA((2 * chunks,)),
+            pltpu.SemaphoreType.DMA((2 * chunks,)),
+        ],
+        compiler_params=pltpu.CompilerParams(
+            collective_id=1, has_side_effects=True, vmem_limit_bytes=60 * 2**20
+        ),
+        name="experts",
+    )(outgoing, w_gate, w_up, w_down, weigh, stream, gain)
+
+
 def local(
     queries,
     key_rows,
@@ -271,27 +429,14 @@
         place, normed, (((0,), (0,)), ((), ())), preferred_element_type=jnp.float32
     ).astype(jnp.bfloat16)
     outgoing = outgoing.reshape(experts_all, capacity, -1)
-    arrived = lax.all_to_all(outgoing, ("sp", "tp"), split_axis=0, concat_axis=0, tiled=True)
-    flat_rows = arrived.reshape(slots_all, -1)
-    gate_act = jnp.dot(flat_rows, w_gate[0], preferred_element_type=jnp.float32)
-    up_act = jnp.dot(flat_rows, w_up[0], preferred_element_type=jnp.float32)
-    hidden = (jax.nn.silu(gate_act) * up_act).astype(jnp.bfloat16)
-    expert_out = jnp.dot(hidden, w_down[0], preferred_element_type=jnp.float32).astype(jnp.bfloat16)
-    returned = lax.all_to_all(
-        expert_out.reshape(experts_all, capacity, -1),
-        ("sp", "tp"),
-        split_axis=0,
-        concat_axis=0,
-        tiled=True,
-    ).reshape(slots_all, -1)
     weigh = sum(
         jnp.where(slot_index[:, k, None] == slot, route_weight[:, k, None], 0.0)
         for k in range(top_count)
     )
-    combined = sum(
-        jnp.dot(part, returned, preferred_element_type=jnp.float32) for part in bf16_parts(weigh)
+    weigh = jnp.stack(bf16_parts(weigh))
+    return experts(
+        outgoing, w_gate[0], w_up[0], w_down[0], weigh, stream, gain_post[None, :], n_tp
     )
-    return (stream_wide + rms_scale(combined, gain_post)).astype(jnp.bfloat16)
 
 
 def solution(mesh):

time: 317 us -> 294 us (0.927); the launches traced: 312 us -> 293 us
  Pallas kernels: 57.2 us -> 210 us
  blocking collectives: 74.7 us -> 0 us
  waiting for transfers between devices: 115 us -> 44.6 us
  matrix products: 28.3 us -> 9.47 us
  starting transfers between devices: 23.4 us -> 17.4 us
    pallas_call x0 -> x1, Pallas kernels: none -> 152 us  [experts(): pl.pallas_call(functools.partial(expert_kernel, n_tp=n_tp, chunks=chunks)...]
    all_to_all x1 -> x0, blocking collectives: 74.7 us -> none  [local(): lax.all_to_all(outgoing, ('sp', 'tp'), split_axis=0, concat_axis=0, tiled...]
    all_to_all x1 -> x0, waiting for transfers between devices: 68.9 us -> none  [local(): lax.all_to_all(expert_out.reshape(experts_all, capacity, -1), ('sp', 'tp'...]
    dot_general x5 -> x0, matrix products: 20.5 us -> none  [the longest x3 9.39 us: local(): jnp.dot(part, returned, preferred_element_type=jnp.float32)]
    all_to_all x1 -> x0, starting transfers between devices: 5.96 us -> none  [local(): lax.all_to_all(expert_out.reshape(experts_all, capacity, -1), ('sp', 'tp'...]
    unnamed x35 -> x28, local copies, waits for them, and re-layouts: 9.11 us -> 7.61 us
  transfers between devices with their start and end apart: 4 -> 3, of which waited for: 3 -> 2; matrix products, arithmetic and copies ran while one was open for 2% -> 2% of each run, Pallas kernels for 8% -> 9%
where the time goes in v1:
time: 294 us; the launch traced here: 293 us
  Pallas kernels  210 us (71%)
  waiting for transfers between devices  44.6 us (15%)
  starting transfers between devices  17.4 us (6%)
  matrix products  9.47 us (3%)
  local copies, waits for them, and re-layouts  8.41 us (3%)
  other arithmetic  3.53 us (1%)
    pallas_call x1, Pallas kernels, experts(): pl.pallas_call(functools.partial(expert_kernel, n_tp=n_tp, chunks=chunks)...  152 us
    pallas_call x2, Pallas kernels, flash(): pl.pallas_call(body, grid=(n_sp,), out_shape=out_shape, in_specs=[q_spec,...  53.9 us
    all_to_all x1, waiting for transfers between devices, local(): got = lax.all_to_all(one, 'sp', split_axis=0, concat_axis=0, tiled=True)  33.5 us
    all_to_all x1, waiting for transfers between devices, local(): lax.all_to_all(out, ('sp', 'tp'), split_axis=0, concat_axis=0, tiled=True)  11 us
    unnamed x28, local copies, waits for them, and re-layouts  7.61 us
    all_to_all x1, starting transfers between devices, local(): lax.all_to_all(out, ('sp', 'tp'), split_axis=0, concat_axis=0, tiled=True)  6.54 us
  transfers between devices with their start and end apart: 3, of which 2 were waited for; matrix products, arithmetic and copies ran while one was open for 2% of the time, Pallas kernels for 9%

profile of v1, /device:TPU:27, one launch (start us, length us, event | category | flops | bytes accessed | tf_op | source)
XLA Modules:
  0.0 293.4 jit_solution(7480064175463261821)
XLA Ops:
  0.0 1.0 copy-done.3
  1.0 1.0 copy-done.4
  2.1 1.0 copy-done.5
  3.1 2.0 pack.1
  5.1 5.4 %all-to-all-start = ((bf16[8,768,128]{2,1,0:T(8,128)(2,1)}), bf16[8,768,128]{2,1,0:T(8,128)(2,1)S(1)}, u32[]{:S(2)}, u32[]{:S(2)}) async-start(bf16[8,768,128]{2,1,0:T(8,128)(2,1)} %get-tuple-element.9), calls=%async_computation | async-start | bytes 3145728 | tf_op jit(solution)/shard_map/all_to_all | solution.py:386
  11.3 1.0 fusion.17
  12.4 33.5 %all-to-all-done.refs_0_.refs_1_ = bf16[8,768,128]{2,1,0:T(8,128)(2,1)S(1)} async-done(((bf16[8,768,128]{2,1,0:T(8,128)(2,1)}), bf16[8,768,128]{2,1,0:T(8,128)(2,1)S(1)}, u32[]{:S(2)}, u32[]{:S(2)}) %all-to-all-start) | async-done | bytes 1572896 | tf_op jit(solution)/shard_map/all_to_all | solution.py:386
  45.9 5.4 %all-to-all-start.1 = ((bf16[8,512,128]{2,1,0:T(8,128)(2,1)}), bf16[8,512,128]{2,1,0:T(8,128)(2,1)S(1)}, u32[]{:S(2)}, u32[]{:S(2)}) async-start(bf16[8,512,128]{2,1,0:T(8,128)(2,1)} %get-tuple-element.12), calls=%async_computation.1 | async-start | bytes 2097152 | tf_op jit(solution)/shard_map/all_to_all | solution.py:388
  51.9 0.5 convolution_convert_fusion.1.refs_2_
  52.4 2.3 convolution_convert_fusion
  54.7 25.9 %flash.2.refs_4_ = f32[4096,128]{1,0:T(8,128)} custom-call(bf16[8,768,128]{2,1,0:T(8,128)(2,1)S(1)} %all-to-all-done.refs_0_.refs_1_, bf16[8,768,128]{2,1,0:T(8,128)(2,1)S(1)} %all-to-all-done.refs_0_.refs_1_, bf16[4096,128]{1,0:T(8,128)(2,1)S(1)} %convolution_convert_fusion.1.refs_2_, bf16[8,1024,128]{2,1,0:T(8,128)(2,1)} %bitcast.23), custom_call_target="tpu_custom_call" | custom-call | flops 9663676416 | bytes 4194304 | tf_op jit(solution)/shard_map/flash/pallas_call | solution.py:190
  80.6 1.2 copy-done.2
  81.8 28.0 %flash.3 = bf16[32,64,128]{2,1,0:T(8,128)(2,1)} custom-call(bf16[8,768,128]{2,1,0:T(8,128)(2,1)} %copy-done, bf16[8,512,128]{2,1,0:T(8,128)(2,1)S(1)} %all-to-all-done.1.refs_1_, bf16[4096,128]{1,0:T(8,128)(2,1)S(1)} %copy-done.2, bf16[8,1024,128]{2,1,0:T(8,128)(2,1)} %bitcast.24, f32[4096,128]{1,0:T(8,128)} %flash.2.refs_4_), custom_call_target="tpu_custom_call" | custom-call | flops 9663676416 | bytes 4194304 | tf_op jit(solution)/shard_map/flash/pallas_call | solution.py:190
  109.8 6.5 %all-to-all-start.2 = ((bf16[32,64,128]{2,1,0:T(8,128)(2,1)}), bf16[32,64,128]{2,1,0:T(8,128)(2,1)S(1)}, u32[]{:S(2)}, u32[]{:S(2)}) async-start(bf16[32,64,128]{2,1,0:T(8,128)(2,1)} %flash.3), calls=%async_computation.2 | async-start | bytes 1048576 | tf_op jit(solution)/shard_map/all_to_all | solution.py:410
  116.4 0.4 reduce-precision_convert_fusion.1
  116.8 1.1 pad_maximum_fusion.weigh_ref
  117.9 11.0 %all-to-all-done.2.in_ref = bf16[32,64,128]{2,1,0:T(8,128)(2,1)S(1)} async-done(((bf16[32,64,128]{2,1,0:T(8,128)(2,1)}), bf16[32,64,128]{2,1,0:T(8,128)(2,1)S(1)}, u32[]{:S(2)}, u32[]{:S(2)}) %all-to-all-start.2) | async-done | bytes 524320 | tf_op jit(solution)/shard_map/all_to_all | solution.py:410
  129.0 0.8 copy-done.7
  129.8 2.1 assemble.1
  131.8 3.8 %multiply_reduce_fusion = (f32[256]{0:T(256)S(1)}, f32[256,2048]{1,0:T(8,128)S(1)}) fusion(bf16[256,1024]{1,0:T(8,128)(2,1)} %assemble.1, bf16[1024,2048]{1,0:T(8,128)(2,1)} %param.19), kind=kOutput, calls=%fused_computation.9 | convolution fusion | flops 1074790144 | bytes 6816768 | tf_op jit(solution)/shard_map/dot_general | solution.py:412
  135.6 0.4 add_convert_fusion.stream_ref
  136.3 2.9 convolution_convert_fusion.2
  139.3 151.9 %experts.1 = bf16[256,2048]{1,0:T(8,128)(2,1)} custom-call(bf16[32,24,2048]{2,1,0:T(8,128)(2,1)} %bitcast.22, bf16[2048,512]{1,0:T(8,128)(2,1)} %bitcast.25, bf16[2048,512]{1,0:T(8,128)(2,1)} %bitcast.26, bf16[512,2048]{1,0:T(8,128)(2,1)} %bitcast.27, bf16[3,256,768]{2,1,0:T(8,128)(2,1)} %pad_maximum_fusion.weigh_ref, bf16[256,2048]{1,0:T(8,128)(2,1)} %copy-done.6, ...), custom_call_target="tpu_custom_call" | custom-call | tf_op jit(solution)/shard_map/experts/pallas_call | solution.py:332
  291.1 2.3 copy.27
  (42 shorter events, 1.6 us)
Async XLA Ops:
  0.0 1.0 copy-start.3
  1.0 1.0 copy-start.4
  2.1 1.0 copy-start.5
  3.1 7.4 %copy-start.10 = (s32[256,2]{0,1:T(2,128)S(1)}, s32[256,2]{0,1:T(2,128)}, u32[]{:S(2)}) copy-start(s32[256,2]{0,1:T(2,128)} %param.23) | copy-start | bytes 6148
  5.1 40.8 %all-to-all-start = ((bf16[8,768,128]{2,1,0:T(8,128)(2,1)}), bf16[8,768,128]{2,1,0:T(8,128)(2,1)S(1)}, u32[]{:S(2)}, u32[]{:S(2)}) async-start(bf16[8,768,128]{2,1,0:T(8,128)(2,1)} %get-tuple-element.9), calls=%async_computation | async-start | bytes 3145728 | tf_op jit(solution)/shard_map/all_to_all | solution.py:386
  45.9 8.8 %copy-start = (bf16[8,768,128]{2,1,0:T(8,128)(2,1)}, bf16[8,768,128]{2,1,0:T(8,128)(2,1)S(1)}, u32[]{:S(2)}) copy-start(bf16[8,768,128]{2,1,0:T(8,128)(2,1)S(1)} %all-to-all-done.refs_0_.refs_1_) | copy-start | bytes 4718596
  45.9 34.6 %all-to-all-start.1 = ((bf16[8,512,128]{2,1,0:T(8,128)(2,1)}), bf16[8,512,128]{2,1,0:T(8,128)(2,1)S(1)}, u32[]{:S(2)}, u32[]{:S(2)}) async-start(bf16[8,512,128]{2,1,0:T(8,128)(2,1)} %get-tuple-element.12), calls=%async_computation.1 | async-start | bytes 2097152 | tf_op jit(solution)/shard_map/all_to_all | solution.py:388
  52.4 2.3 copy-start.1
  80.6 1.2 copy-start.2
  81.8 34.6 %copy-start.11 = (f32[256,2]{0,1:T(2,128)S(1)}, f32[256,2]{0,1:T(2,128)}, u32[]{:S(2)}) copy-start(f32[256,2]{0,1:T(2,128)} %param.24) | copy-start | bytes 6148
  109.8 19.1 %all-to-all-start.2 = ((bf16[32,64,128]{2,1,0:T(8,128)(2,1)}), bf16[32,64,128]{2,1,0:T(8,128)(2,1)S(1)}, u32[]{:S(2)}, u32[]{:S(2)}) async-start(bf16[32,64,128]{2,1,0:T(8,128)(2,1)} %flash.3), calls=%async_computation.2 | async-start | bytes 1048576 | tf_op jit(solution)/shard_map/all_to_all | solution.py:410
  129.0 0.8 copy-start.7
  131.8 3.8 %copy-start.8 = (bf16[256,2048]{1,0:T(8,128)(2,1)S(1)}, bf16[256,2048]{1,0:T(8,128)(2,1)}, u32[]{:S(2)}) copy-start(bf16[256,2048]{1,0:T(8,128)(2,1)} %param.18) | copy-start | bytes 3145732
  131.8 3.8 %copy-start.9 = (f32[2048]{0:T(1024)S(1)}, f32[2048]{0:T(1024)}, u32[]{:S(2)}) copy-start(f32[2048]{0:T(1024)} %param.20) | copy-start | bytes 24580
  135.6 0.7 copy-start.12
  136.0 3.2 %copy-start.6 = (bf16[256,2048]{1,0:T(8,128)(2,1)}, bf16[256,2048]{1,0:T(8,128)(2,1)S(1)}, u32[]{:S(2)}) copy-start(bf16[256,2048]{1,0:T(8,128)(2,1)S(1)} %add_convert_fusion.stream_ref) | copy-start | bytes 3145732

commit v2 on v1

--- a/solution.py
+++ b/solution.py
@@ -14,6 +14,7 @@
 MESH = pl.DeviceIdType.MESH
 CHUNKS = 4
 GROUPS = 4
+KEY_PARTS = 1
 
 
 def rms_scale(rows, gain):
@@ -30,31 +31,29 @@
     return parts
 
 
-def pack_kernel(q_ref, k_ref, v_ref, one_ref, two_ref, *, shares, n_tp):
+def pack_kernel(q_ref, k_ref, v_ref, kv_out, q_out, *, shares, n_tp):
     tok_dev, width = q_ref.shape
-    first = tok_dev - two_ref.shape[1]
     rows_dev = tok_dev // n_tp
     sub = rows_dev // shares
     for h in range(width // HEAD_DIM):
         cols = pl.ds(h * HEAD_DIM, HEAD_DIM)
-        pairs = jnp.concatenate((k_ref[:, cols], v_ref[:, cols]), axis=1)
+        kv_out[h] = jnp.concatenate((k_ref[:, cols], v_ref[:, cols]), axis=1)
         for r in range(shares):
-            dest = h * shares + r
-            one_ref[dest, :first] = pairs[:first]
-            two_ref[dest] = pairs[first:]
             for t in range(n_tp // 2):
                 low, high = (
                     q_ref[pl.ds((t + step) * rows_dev + r * sub, sub), cols]
                     for step in (0, n_tp // 2)
                 )
-                one_ref[dest, pl.ds(first + t * sub, sub)] = jnp.concatenate((low, high), axis=1)
-
-
-def pack(queries, key_rows, value_rows, first, shares, n_tp):
+                q_out[h * shares + r, pl.ds(t * sub, sub)] = jnp.concatenate((low, high), axis=1)
+
+
+def pack(queries, key_rows, value_rows, shares, n_tp):
     tok_dev, width = queries.shape
-    dests = width // HEAD_DIM * shares
-    half = tok_dev // shares // 2
-    shapes = [(dests, first + half, 2 * HEAD_DIM), (dests, tok_dev - first, 2 * HEAD_DIM)]
+    heads = width // HEAD_DIM
+    shapes = [
+        (heads, tok_dev, 2 * HEAD_DIM),
+        (heads * shares, tok_dev // shares // 2, 2 * HEAD_DIM),
+    ]
     return pl.pallas_call(
         functools.partial(pack_kernel, shares=shares, n_tp=n_tp),
         out_shape=[jax.ShapeDtypeStruct(shape, jnp.bfloat16) for shape in shapes],
@@ -65,141 +64,257 @@
     )(queries, key_rows, value_rows)
 
 
-def assemble_kernel(in_ref, out_ref, *, shares, n_tp, local_heads):
-    half = in_ref.shape[1]
+def attend_kernel(
+    kv_ref, q_ref, side_q_ref, side_k_ref, o_ref,
+    kv_all, q_all, k_aug, v_aug, q_aug, peak_ref, acc_ref, out_ref, heads_ref,
+    own_sem, q_sem, kv_sem, head_sem, send_sem, *, n_tp, local_heads,
+):
+    groups = local_heads
+    n_sp = q_ref.shape[0]
+    shares = n_sp // groups
+    tok_dev = kv_ref.shape[1]
+    chunk = 2 * q_ref.shape[1]
+    sub = chunk // n_tp
+    rows_dev = sub * shares
+    lanes = 2 * HEAD_DIM
+    n = n_sp * n_tp
+    sp, tp = lax.axis_index("sp"), lax.axis_index("tp")
+    me = sp * n_tp + tp
+    group, rank = sp // shares, lax.rem(sp, shares)
+
+    def plane(s):
+        down = jnp.where(s <= group, group - s, s)
+        up = jnp.where(s <= groups - 1 - group, group + s, groups - 1 - s)
+        return jnp.where(2 * group < groups, down, up)
+
+    def block_at(i):
+        return plane(i // shares) * shares + lax.rem(rank + lax.rem(i, shares), shares)
+
+    barrier = pltpu.get_barrier_semaphore()
+
+    def greet(o, carry):
+        d = lax.rem(me + o, n)
+        where = (d // n_tp, lax.rem(d, n_tp))
+        pl.semaphore_signal(barrier, inc=1, device_id=where, device_id_type=MESH)
+        return carry
+
+    lax.fori_loop(1, n, greet, 0)
+    own_kv = pltpu.make_async_copy(kv_ref.at[group], kv_all.at[sp], own_sem.at[0])
+    own_q = pltpu.make_async_copy(q_ref.at[sp], q_all.at[sp], own_sem.at[1])
+    own_kv.start()
+    own_q.start()
+    pl.semaphore_wait(barrier, n - 1)
+
+    def kv_copy(src, block, dest, slot):
+        return pltpu.make_async_remote_copy(
+            src_ref=src, dst_ref=kv_all.at[block],
+            send_sem=send_sem.at[slot], recv_sem=kv_sem.at[block],
+            device_id=(dest, tp), device_id_type=MESH,
+        )
+
+    def q_copy(src, block, dest):
+        return pltpu.make_async_remote_copy(
+            src_ref=src, dst_ref=q_all.at[block],
+            send_sem=send_sem.at[0], recv_sem=q_sem.at[block],
+            device_id=(dest, tp), device_id_type=MESH,
+        )
+
+    for s in range(groups):
+        for k in range(shares):
+            dest = block_at(s * shares + k)
+            if s or k:
+                q_copy(q_ref.at[dest], sp, dest).start()
+            if s == 0 and k:
+                kv_copy(kv_ref.at[group], sp, dest, 1).start()
+            if s and k == 0:
+                kv_copy(kv_ref.at[plane(s)], sp, dest, 2).start()
+
+    row = lax.broadcasted_iota(jnp.int32, (chunk, 1), 0)
+    pos = row // sub * rows_dev + rank * sub + lax.rem(row, sub)
+
+    def build(block):
+        lane = lax.broadcasted_iota(jnp.int32, (tok_dev, lanes), 1)
+        kv = kv_all[block].astype(jnp.float32)
+        side = side_k_ref[block].astype(jnp.float32)
+        k_aug[block] = jnp.where(lane < HEAD_DIM, kv, side).astype(jnp.bfloat16)
+        ones = (lane == 0).astype(jnp.float32)
+        v_aug[block] = jnp.where(lane < HEAD_DIM, ones, kv).astype(jnp.bfloat16)
+        packed = q_all[block]
+        queries = jnp.concatenate((packed[:, :HEAD_DIM], packed[:, HEAD_DIM:]), axis=0)
+        queries = queries * jnp.bfloat16(HEAD_DIM**-0.5)
+        side = side_q_ref[pl.ds(pl.multiple_of(block * chunk, chunk), chunk), HEAD_DIM:]
+        q_aug[block] = jnp.concatenate((queries, side), axis=1)
+        peak_ref[block] = jnp.full((chunk, lanes), MASKED, jnp.float32)
+        acc_ref[block] = jnp.zeros((chunk, lanes), jnp.float32)
+
+    def step(i, j, masked):
+        for part in range(KEY_PARTS):
+            count = tok_dev // KEY_PARTS
+            keys = pl.ds(part * count, count)
+            scores = lax.dot_general(
+                q_aug[i], k_aug[j, keys], (((1,), (1,)), ((), ())),
+                preferred_element_type=jnp.float32,
+            )
+            if masked:
+                key = part * count + lax.broadcasted_iota(jnp.int32, (1, count), 1)
+                scores = jnp.where(key <= pos, scores, MASKED)
+            before = peak_ref[i]
+            peak = jnp.maximum(before, jnp.max(scores, axis=1, keepdims=True))
+            probs = jnp.exp(scores - jnp.concatenate([peak] * (count // lanes), axis=1)).astype(jnp.bfloat16)
+            peak_ref[i] = peak
+            acc_ref[i] = acc_ref[i] * jnp.exp(before - peak) + jnp.dot(
+                probs, v_aug[j, keys], preferred_element_type=jnp.float32
+            )
+
+    def head_copy(block, t):
+        slot = block * n_tp + t
+        return pltpu.make_async_remote_copy(
+            src_ref=out_ref.at[slot], dst_ref=heads_ref.at[me],
+            send_sem=send_sem.at[4], recv_sem=head_sem,
+            device_id=(block, t), device_id_type=MESH,
+        )
+
+    own_head = pltpu.make_async_copy(out_ref.at[me], heads_ref.at[me], own_sem.at[2])
+
+    def finish(block):
+        acc = acc_ref[block]
+        out = acc[:, HEAD_DIM:] / acc[:, :1]
+        half = sub // 2
+        for t in range(n_tp):
+            top, low = (out[t * sub + at : t * sub + at + half] for at in (0, half))
+            out_ref[block * n_tp + t] = jnp.concatenate((top, low), axis=1).astype(jnp.bfloat16)
+        for t in range(n_tp):
+            mine = (block == sp) & (tp == t)
+
+            @pl.when(mine)
+            def _():
+                own_head.start()
+
+            @pl.when(jnp.logical_not(mine))
+            def _(t=t):
+                head_copy(block, t).start()
+
+    def relay(i):
+        block = block_at(i)
+        kv_copy(kv_all.at[block], block, block, 3).wait_recv()
+        for k in range(1, shares):
+            dest = group * shares + lax.rem(rank + k, shares)
+            kv_copy(kv_all.at[block], block, dest, 3).start()
+
+    def one_block(i, carry):
+        block = block_at(i)
+        s, k = i // shares, lax.rem(i, shares)
+        turn = k == shares - 1
+
+        @pl.when(i == 0)
+        def _():
+            own_kv.wait()
+            own_q.wait()
+
+        @pl.when(i > 0)
+        def _():
+            q_copy(q_all.at[block], block, block).wait_recv()
+
+        @pl.when(k > 0)
+        def _():
+            kv_copy(kv_all.at[block], block, block, 3).wait_recv()
+
+        @pl.when(turn & (s > 0) & (s < groups - 1))
+        def _():
+            relay(i + 1)
+
+        build(block)
+
+        def pair(m, carry):
+            other = block_at(m)
+            step(jnp.maximum(block, other), jnp.minimum(block, other), False)
+
+            @pl.when(i == n_sp - 1)
+            def _():
+                finish(other)
+
+            return carry
+
+        lax.fori_loop(0, i, pair, 0)
+        step(block, block, True)
+
+        @pl.when(turn & (s == 0) & (groups > 1))
+        def _():
+            relay(i + 1)
+
+        return carry
+
+    lax.fori_loop(0, n_sp, one_block, 0)
+    finish(block_at(n_sp - 1))
+    own_head.wait()
+
+    def sent(buf, count, slot):
+        if count:
+            pltpu.make_async_remote_copy(
+                src_ref=buf.at[pl.ds(0, count)], dst_ref=buf.at[pl.ds(0, count)],
+                send_sem=send_sem.at[slot], recv_sem=head_sem,
+                device_id=(sp, tp), device_id_type=MESH,
+            ).wait_send()
+
+    pltpu.make_async_remote_copy(
+        src_ref=heads_ref.at[pl.ds(0, n - 1)], dst_ref=heads_ref.at[pl.ds(0, n - 1)],
+        send_sem=send_sem.at[4], recv_sem=head_sem,
+        device_id=(sp, tp), device_id_type=MESH,
+    ).wait_recv()
+    half = sub // 2
     for t in range(n_tp):
         for h in range(0, local_heads, 2):
             for r in range(shares):
-                left = in_ref[(h * shares + r) * n_tp + t]
-                right = in_ref[((h + 1) * shares + r) * n_tp + t]
+                left = heads_ref[(h * shares + r) * n_tp + t]
+                right = heads_ref[((h + 1) * shares + r) * n_tp + t]
                 for part in range(2):
                     cols = slice(part * HEAD_DIM, (part + 1) * HEAD_DIM)
-                    out_ref[
+                    o_ref[
                         pl.ds((2 * r + part) * half, half),
                         pl.ds((t * local_heads + h) * HEAD_DIM, 2 * HEAD_DIM),
                     ] = jnp.concatenate((left[:, cols], right[:, cols]), axis=1)
-
-
-def assemble(heads, shares, n_tp, local_heads):
-    shape = (2 * shares * heads.shape[1], n_tp * local_heads * HEAD_DIM)
+    sent(q_ref, n_sp - 1, 0)
+    sent(kv_all, shares - 1, 1)
+    sent(kv_all, groups - 1, 2)
+    sent(kv_all, (groups - 1) * (shares - 1), 3)
+    sent(out_ref, n - 1, 4)
+
+
+def attend(kv, q, side_q, side_k, n_tp):
+    local_heads, tok_dev, lanes = kv.shape
+    n_sp, half_chunk = q.shape[:2]
+    chunk = 2 * half_chunk
+    n = n_sp * n_tp
+    sub = chunk // n_tp
+    bf16, f32 = jnp.bfloat16, jnp.float32
+    vmem = pl.BlockSpec(memory_space=pltpu.VMEM)
+    rows_dev = tok_dev // n_tp
     return pl.pallas_call(
-        functools.partial(
-            assemble_kernel, shares=shares, n_tp=n_tp, local_heads=local_heads
+        functools.partial(attend_kernel, n_tp=n_tp, local_heads=local_heads),
+        out_shape=jax.ShapeDtypeStruct((rows_dev, n_tp * local_heads * HEAD_DIM), bf16),
+        in_specs=[vmem] * 4,
+        out_specs=vmem,
+        scratch_shapes=[
+            pltpu.VMEM((n_sp, tok_dev, lanes), bf16),
+            pltpu.VMEM((n_sp, half_chunk, lanes), bf16),
+            pltpu.VMEM((n_sp, tok_dev, lanes), bf16),
+            pltpu.VMEM((n_sp, tok_dev, lanes), bf16),
+            pltpu.VMEM((n_sp, chunk, lanes), bf16),
+            pltpu.VMEM((n_sp, chunk, lanes), f32),
+            pltpu.VMEM((n_sp, chunk, lanes), f32),
+            pltpu.VMEM((n, sub // 2, lanes), bf16),
+            pltpu.VMEM((n, sub // 2, lanes), bf16),
+            pltpu.SemaphoreType.DMA((3,)),
+            pltpu.SemaphoreType.DMA((n_sp,)),
+            pltpu.SemaphoreType.DMA((n_sp,)),
+            pltpu.SemaphoreType.DMA,
+            pltpu.SemaphoreType.DMA((5,)),
+        ],
+        compiler_params=pltpu.CompilerParams(
+            collective_id=0, has_side_effects=True, vmem_limit_bytes=56 * 2**20
         ),
-        out_shape=jax.ShapeDtypeStruct(shape, jnp.bfloat16),
-        in_specs=[pl.BlockSpec(memory_space=pltpu.VMEM)],
-        out_specs=pl.BlockSpec(memory_space=pltpu.VMEM),
-        name="assemble",
-    )(heads)
-
-
-def flash_kernel(*refs, begun, span, shares, sub, rows_dev, n_tp):
-    if begun:
-        q_ref, kv_ref, side_q_ref, side_k_ref, state_ref, o_ref, k_aug, v_aug = refs
-    else:
-        q_ref, kv_ref, side_q_ref, side_k_ref, o_ref, k_aug, v_aug = refs
-    lo, hi = span
-    count = hi - lo
-    tile = pl.program_id(0)
-    rank = lax.rem(lax.axis_index("sp"), shares)
-
-    @pl.when(tile == 0)
-    def _():
-        lane = lax.broadcasted_iota(jnp.int32, (count, 2 * HEAD_DIM), 1)
-
-        def one(src, carry):
-            kv = kv_ref[src, :count].astype(jnp.float32)
-            side = side_k_ref[src, lo:hi].astype(jnp.float32)
-            k_aug[src] = jnp.where(lane < HEAD_DIM, kv, side).astype(jnp.bfloat16)
-            ones = (lane == 0).astype(jnp.float32)
-            v_aug[src] = jnp.where(lane < HEAD_DIM, ones, kv).astype(jnp.bfloat16)
-            return carry
-
-        lax.fori_loop(0, kv_ref.shape[0], one, 0)
-
-    packed = q_ref[0]
-    queries = jnp.concatenate((packed[:, :HEAD_DIM], packed[:, HEAD_DIM:]), axis=0)
-    queries = queries * jnp.bfloat16(HEAD_DIM**-0.5)
-    queries = jnp.concatenate((queries, side_q_ref[:, HEAD_DIM:]), axis=1)
-    rows = queries.shape[0]
-    out_lane = lax.broadcasted_iota(jnp.int32, (rows, 2 * HEAD_DIM), 1)
-
-    def step(src, state, masked):
-        peak, acc = state
-        scores = lax.dot_general(
-            queries, k_aug[src], (((1,), (1,)), ((), ())), preferred_element_type=jnp.float32
-        )
-        if masked:
-            row = lax.broadcasted_iota(jnp.int32, (rows, 1), 0)
-            pos = row // sub * rows_dev + rank * sub + row % sub
-            key = lo + lax.broadcasted_iota(jnp.int32, (1, count), 1)
-            scores = jnp.where(key <= pos, scores, MASKED)
-        new_peak = jnp.maximum(peak, jnp.max(scores, axis=1, keepdims=True))
-        probs = jnp.exp(scores - new_peak).astype(jnp.bfloat16)
-        acc = acc * jnp.exp(peak - new_peak) + jnp.dot(
-            probs, v_aug[src], preferred_element_type=jnp.float32
-        )
-        return new_peak, acc
-
-    if begun:
-        before = state_ref[...]
-        kept = jnp.max(jnp.where(out_lane == 1, before, -jnp.inf), axis=1, keepdims=True)
-        state = (kept, jnp.where(out_lane == 1, 0.0, before))
-    else:
-        state = (
-            jnp.full((rows, 1), MASKED, jnp.float32),
-            jnp.zeros((rows, 2 * HEAD_DIM), jnp.float32),
-        )
-    state = lax.fori_loop(0, tile, lambda i, state: step(i, state, False), state)
-    peak, acc = step(tile, state, True)
-    if not begun:
-        o_ref[...] = jnp.where(out_lane == 1, peak, acc)
-        return
-    out = acc[:, HEAD_DIM:] / acc[:, :1]
-    half = sub // 2
-    for t in range(n_tp):
-        top, low = (out[t * sub + step : t * sub + step + half] for step in (0, half))
-        o_ref[t] = jnp.concatenate((top, low), axis=1).astype(o_ref.dtype)
-
-
-def flash(got, kv, side_q, side_k, state, span, first, sub, rows_dev, n_tp, shares):
-    n_sp, count = kv.shape[0], span[1] - span[0]
-    chunk = n_tp * sub
-    lanes = 2 * HEAD_DIM
-    whole = pl.BlockSpec(memory_space=pltpu.VMEM)
-    begun = state is not None
-    wide = pl.BlockSpec((chunk, lanes), lambda i: (i, 0))
-    if begun:
-        out_shape = jax.ShapeDtypeStruct((n_sp * n_tp, sub // 2, lanes), jnp.bfloat16)
-        out_spec = pl.BlockSpec((n_tp, sub // 2, lanes), lambda i: (i, 0, 0))
-    else:
-        out_shape = jax.ShapeDtypeStruct((n_sp * chunk, lanes), jnp.float32)
-        out_spec = wide
-    first_q = first // (chunk // 2)
-    body = functools.partial(
-        flash_kernel,
-        begun=begun,
-        span=span,
-        shares=shares,
-        sub=sub,
-        rows_dev=rows_dev,
-        n_tp=n_tp,
-    )
-    q_spec = pl.BlockSpec((1, chunk // 2, lanes), lambda i: (i, first_q, 0))
-    pairs = n_sp * (n_sp + 1) // 2 * chunk * count
-    return pl.pallas_call(
-        body,
-        grid=(n_sp,),
-        out_shape=out_shape,
-        in_specs=[q_spec, whole, wide, whole] + [wide] * begun,
-        out_specs=out_spec,
-        scratch_shapes=[pltpu.VMEM((n_sp, count, lanes), jnp.bfloat16)] * 2,
-        compiler_params=pltpu.CompilerParams(vmem_limit_bytes=50 * 2**20),
-        cost_estimate=pl.CostEstimate(
-            flops=8 * lanes * pairs, bytes_accessed=2**22, transcendentals=pairs
-        ),
-        name="flash",
-    )(got, kv, side_q, side_k, *([state] if begun else []))
+        name="attend",
+    )(kv, q, side_q, side_k)
 
 
 def expert_kernel(
@@ -380,12 +495,7 @@
     rows_dev = residual.shape[0]
     sub = rows_dev // shares
     chunk = n_tp * sub
-    half = chunk // 2
-    first = tok_dev * 5 // 8 // half * half
-    one, two = pack(queries, key_rows, value_rows, first, shares, n_tp)
-    got = lax.all_to_all(one, "sp", split_axis=0, concat_axis=0, tiled=True)
-    got, two = lax.optimization_barrier((got, two))
-    got_two = lax.all_to_all(two, "sp", split_axis=0, concat_axis=0, tiled=True)
+    kv, q = pack(queries, key_rows, value_rows, shares, n_tp)
 
     me = lax.axis_index("sp")
     gate = lax.dynamic_index_in_dim(cum_gate, me // shares, 0, keepdims=False)
@@ -404,11 +514,7 @@
     side_q = side_lanes(bf16_parts(gate_q) + [ones_q] * 3)
     side_k = side_lanes([ones_k] * 3 + bf16_parts(-gate))
     side_k = side_k.reshape(n_sp, tok_dev, 2 * HEAD_DIM)
-    fixed = (first, sub, rows_dev, n_tp, shares)
-    state = flash(got, got, side_q, side_k, None, (0, first), *fixed)
-    out = flash(got, got_two, side_q, side_k, state, (first, tok_dev), *fixed)
-    heads = lax.all_to_all(out, ("sp", "tp"), split_axis=0, concat_axis=0, tiled=True)
-    head_rows = assemble(heads, shares, n_tp, local_heads)
+    head_rows = attend(kv, q, side_q, side_k, n_tp)
     projected = jnp.dot(head_rows, out_weight, preferred_element_type=jnp.float32)
     stream = (residual.astype(jnp.float32) + rms_scale(projected, gain_mix)).astype(jnp.bfloat16)
     stream_wide = lax.optimization_barrier(stream).astype(jnp.float32)

time: 294 us -> 249 us (0.85)
  waiting for transfers between devices: 44.6 us -> 0 us
  Pallas kernels: 210 us -> 228 us
  starting transfers between devices: 17.4 us -> 0 us
    all_to_all x3 -> x0, waiting for transfers between devices: 44.6 us -> none  [the longest x1 33.5 us: local(): got = lax.all_to_all(one, 'sp', split_axis=0, concat_axis=0, tiled=True)]
    pallas_call x3 -> x1, Pallas kernels: 56 us -> 76.3 us  [attend(): pl.pallas_call(functools.partial(attend_kernel, n_tp=n_tp, local_heads=lo...]
    all_to_all x3 -> x0, starting transfers between devices: 17.4 us -> none  [the longest x1 6.54 us: local(): lax.all_to_all(out, ('sp', 'tp'), split_axis=0, concat_axis=0, tiled=True)]
    unnamed x28 -> x22, local copies, waits for them, and re-layouts: 7.61 us -> 4.92 us
  transfers between devices with their start and end apart: 3 -> 0, of which waited for: 2 -> 0; matrix products, arithmetic and copies ran while one was open for 2% -> 0% of each run, Pallas kernels for 9% -> 0%
where the time goes in v2:
time: 249 us
  Pallas kernels  228 us (92%)
  matrix products  9.14 us (4%)
  local copies, waits for them, and re-layouts  6.47 us (3%)
  other arithmetic  4.25 us (2%)
    pallas_call x1, Pallas kernels, experts(): pl.pallas_call(functools.partial(expert_kernel, n_tp=n_tp, chunks=chunks)...  152 us
    pallas_call x1, Pallas kernels, attend(): pl.pallas_call(functools.partial(attend_kernel, n_tp=n_tp, local_heads=lo...  76.3 us

profile of v2, /device:TPU:27, one launch (start us, length us, event | category | flops | bytes accessed | tf_op | source)
XLA Modules:
  0.0 248.5 jit_solution(2236300013651907090)
XLA Ops:
  0.0 0.8 fusion.22
  0.8 1.0 fusion.17
  1.8 0.1 stack.11
  2.1 0.2 stack.13
  2.3 0.8 copy.24
  3.1 0.1 eq.122
  3.3 0.3 convert_reduce_fusion
  3.6 0.1 reduce_sum.30
  3.7 0.1 copy.25
  3.8 0.7 multiply_add_fusion
  4.5 1.5 convolution_convert_fusion.1.side_q_ref
  6.0 0.4 reduce-precision_convert_fusion.1
  6.4 1.2 pad_maximum_fusion.weigh_ref
  7.6 0.5 pack.1
  8.0 1.0 copy-done
  9.0 0.8 copy-done.4
  9.8 2.3 convolution_convert_fusion
  12.1 76.3 %attend.1 = bf16[256,1024]{1,0:T(8,128)(2,1)} custom-call(bf16[4,1024,128]{2,1,0:T(8,128)(2,1)} %copy-done, bf16[8,256,128]{2,1,0:T(8,128)(2,1)} %copy-done.4, bf16[4096,128]{1,0:T(8,128)(2,1)} %convolution_convert_fusion.1.side_q_ref, bf16[8,1024,128]{2,1,0:T(8,128)(2,1)} %bitcast.22), custom_call_target="tpu_custom_call" | custom-call | tf_op jit(solution)/shard_map/attend/pallas_call | solution.py:292
  88.4 2.5 multiply_reduce_fusion
  91.0 0.4 add_convert_fusion.stream_ref
  91.3 0.3 fusion
  91.7 2.9 %convolution_convert_fusion.2 = bf16[768,2048]{1,0:T(8,128)(2,1)} fusion(bf16[256,2048]{1,0:T(8,128)(2,1)S(1)} %add_convert_fusion.stream_ref, f32[2048]{0:T(1024)S(1)} %copy-done.9, f32[256]{0:T(256)S(1)} %add_rsqrt_fusion, s32[256]{0:T(256)S(1)} %bitcast.34, s32[256]{0:T(256)S(1)} %bitcast.32), kind=kOutput, calls=%fused_computation.2 | convolution fusion | flops 810549248 | bytes 4205568 | tf_op jit(solution)/shard_map/dot_general | solution.py:534
  94.6 151.7 %experts.1 = bf16[256,2048]{1,0:T(8,128)(2,1)} custom-call(bf16[32,24,2048]{2,1,0:T(8,128)(2,1)} %bitcast.23, bf16[2048,512]{1,0:T(8,128)(2,1)} %bitcast.24, bf16[2048,512]{1,0:T(8,128)(2,1)} %bitcast.25, bf16[512,2048]{1,0:T(8,128)(2,1)} %bitcast.26, bf16[3,256,768]{2,1,0:T(8,128)(2,1)} %pad_maximum_fusion.weigh_ref, bf16[256,2048]{1,0:T(8,128)(2,1)} %copy-done.5, ...), custom_call_target="tpu_custom_call" | custom-call | tf_op jit(solution)/shard_map/experts/pallas_call | solution.py:447
  246.2 2.3 copy.27
  (28 shorter events, 0.2 us)
Async XLA Ops:
  4.5 3.1 %copy-start.1 = (bf16[1024,256]{1,0:T(8,128)(2,1)S(1)}, bf16[1024,256]{1,0:T(8,128)(2,1)}, u32[]{:S(2)}) copy-start(bf16[1024,256]{1,0:T(8,128)(2,1)} %q_ref.1) | copy-start | bytes 1572868
  4.5 3.1 %copy-start.2 = (bf16[1024,256]{1,0:T(8,128)(2,1)S(1)}, bf16[1024,256]{1,0:T(8,128)(2,1)}, u32[]{:S(2)}) copy-start(bf16[1024,256]{1,0:T(8,128)(2,1)} %k_ref.1) | copy-start | bytes 1572868
  4.5 3.1 %copy-start.3 = (bf16[1024,256]{1,0:T(8,128)(2,1)S(1)}, bf16[1024,256]{1,0:T(8,128)(2,1)}, u32[]{:S(2)}) copy-start(bf16[1024,256]{1,0:T(8,128)(2,1)} %v_ref.1) | copy-start | bytes 1572868
  8.0 1.0 copy-start
  9.0 0.8 copy-start.4
  12.1 76.3 %copy-start.8 = (bf16[1024,2048]{1,0:T(8,128)(2,1)S(1)}, bf16[1024,2048]{1,0:T(8,128)(2,1)}, u32[]{:S(2)}) copy-start(bf16[1024,2048]{1,0:T(8,128)(2,1)} %param.19) | copy-start | bytes 12582916
  88.4 2.5 %copy-start.6 = (bf16[256,2048]{1,0:T(8,128)(2,1)S(1)}, bf16[256,2048]{1,0:T(8,128)(2,1)}, u32[]{:S(2)}) copy-start(bf16[256,2048]{1,0:T(8,128)(2,1)} %param.18) | copy-start | bytes 3145732
  88.4 2.5 %copy-start.7 = (f32[2048]{0:T(1024)S(1)}, f32[2048]{0:T(1024)}, u32[]{:S(2)}) copy-start(f32[2048]{0:T(1024)} %param.20) | copy-start | bytes 24580
  90.9 0.7 copy-start.9
  91.3 3.2 %copy-start.5 = (bf16[256,2048]{1,0:T(8,128)(2,1)}, bf16[256,2048]{1,0:T(8,128)(2,1)S(1)}, u32[]{:S(2)}) copy-start(bf16[256,2048]{1,0:T(8,128)(2,1)S(1)} %add_convert_fusion.stream_ref) | copy-start | bytes 3145732

commit v3 on v2

--- a/solution.py
+++ b/solution.py
@@ -15,11 +15,7 @@
 CHUNKS = 4
 GROUPS = 4
 KEY_PARTS = 1
-
-
-def rms_scale(rows, gain):
-    mean_sq = jnp.mean(rows * rows, axis=-1, keepdims=True)
-    return rows * lax.rsqrt(mean_sq + NORM_EPS) * gain
+WEIGH_COLS = 256
 
 
 def bf16_parts(values):
@@ -318,12 +314,19 @@
 
 
 def expert_kernel(
-    out_ref, wg_hbm, wu_hbm, wd_hbm, weigh_ref, stream_ref, gain_ref, o_ref,
-    arrived, made, returned, wg, wu, wd, gate_acc, up_acc, hidden, comb,
-    w_sem, own_sem, send_sem, recv_sem, *, n_tp, chunks,
+    heads_ref, ow_ref, res_ref, gains_ref, ids_ref, weight_ref, wg_hbm, wu_hbm, wd_hbm, o_ref,
+    sent, arrived, made, returned, wg, wu, wd, gate_acc, up_acc, hidden, comb, stream, normed, weigh,
+    w_sem, own_sem, send_sem, recv_sem, *, n_tp, chunks, tight,
 ):
-    n, cap, width = out_ref.shape
+    n, cap, width = sent.shape
+    rows_dev = stream.shape[0]
     part = width // chunks
+    last = chunks - 1
+    fold = chunks == 4 and cap - tight == 2 and tight > 8
+    keep = cap - 8
+    group = n // GROUPS
+    rows = group * cap
+    f32, bf16 = jnp.float32, jnp.bfloat16
     sp, tp = lax.axis_index("sp"), lax.axis_index("tp")
     me = sp * n_tp + tp
 
@@ -345,17 +348,55 @@
         return carry
 
     lax.fori_loop(1, n, greet, 0)
-    pl.semaphore_wait(barrier, n - 1)
 
     def cols(c):
         return pl.ds(c * part, part)
+
+    expert = lax.broadcasted_iota(jnp.int32, (n, rows_dev), 0)
+    tri = (
+        lax.broadcasted_iota(jnp.int32, (rows_dev, rows_dev), 0)
+        < lax.broadcasted_iota(jnp.int32, (rows_dev, rows_dev), 1)
+    ).astype(f32).astype(bf16)
+    taken = jnp.zeros((n, 1), f32)
+    slots = []
+    for k in range(ids_ref.shape[0]):
+        ids = ids_ref[pl.ds(k, 1), :]
+        named = (expert == ids).astype(f32)
+        ahead = jnp.dot(named.astype(bf16), tri, preferred_element_type=f32) + taken
+        rank = jnp.sum(named * ahead, axis=0, keepdims=True)
+        taken = taken + jnp.sum(named, axis=1, keepdims=True)
+        slots.append(ids * cap + rank.astype(jnp.int32))
+
+    heads = heads_ref[...]
+    total = jnp.zeros((rows_dev, 1), f32)
+    for c in range(chunks):
+        proj = jnp.dot(heads, ow_ref[:, cols(c)], preferred_element_type=f32)
+        comb[:, cols(c)] = proj
+        total = total + jnp.sum(proj * proj, axis=1, keepdims=True)
+    scale = lax.rsqrt(total / width + NORM_EPS)
+    total = jnp.zeros((rows_dev, 1), f32)
+    for c in range(chunks):
+        wide = res_ref[:, cols(c)].astype(f32) + comb[:, cols(c)] * scale * gains_ref[pl.ds(0, 1), cols(c)]
+        stream[:, cols(c)] = wide.astype(bf16)
+        wide = stream[:, cols(c)].astype(f32)
+        total = total + jnp.sum(wide * wide, axis=1, keepdims=True)
+    scale = lax.rsqrt(total / width + NORM_EPS)
+    for c in range(chunks):
+        wide = stream[:, cols(c)].astype(f32)
+        normed[:, cols(c)] = (wide * scale * gains_ref[pl.ds(1, 1), cols(c)]).astype(bf16)
+    pl.semaphore_wait(barrier, n - 1)
+
+    def window(ref, at, c):
+        if fold and c == last:
+            return ref.at[at, pl.ds(0, keep), cols(c)]
+        return ref.at[at, :, cols(c)]
 
     def send_all(src, dst, c, slot):
         def one(o, carry):
             d, where = peer(o)
             pltpu.make_async_remote_copy(
-                src_ref=src.at[d, :, cols(c)],
-                dst_ref=dst.at[me, :, cols(c)],
+                src_ref=window(src, d, c),
+                dst_ref=window(dst, me, c),
                 send_sem=send_sem.at[slot],
                 recv_sem=recv_sem.at[slot],
                 device_id=where,
@@ -363,13 +404,13 @@
             ).start()
             return carry
 
-        pltpu.make_async_copy(src.at[me, :, cols(c)], dst.at[me, :, cols(c)], own_sem.at[slot]).start()
+        pltpu.make_async_copy(window(src, me, c), window(dst, me, c), own_sem.at[slot]).start()
         lax.fori_loop(1, n, one, 0)
 
     def all_copies(src, dst, c, slot):
         return pltpu.make_async_remote_copy(
-            src_ref=src.at[pl.ds(0, n - 1), :, cols(c)],
-            dst_ref=dst.at[pl.ds(0, n - 1), :, cols(c)],
+            src_ref=window(src, pl.ds(0, n - 1), c),
+            dst_ref=window(dst, pl.ds(0, n - 1), c),
             send_sem=send_sem.at[slot],
             recv_sem=recv_sem.at[slot],
             device_id=peer(1)[1],
@@ -377,67 +418,128 @@
         )
 
     def wait_all(src, dst, c, slot):
-        pltpu.make_async_copy(src.at[me, :, cols(c)], dst.at[me, :, cols(c)], own_sem.at[slot]).wait()
+        pltpu.make_async_copy(window(src, me, c), window(dst, me, c), own_sem.at[slot]).wait()
         all_copies(src, dst, c, slot).wait_recv()
 
+    spare = lax.broadcasted_iota(jnp.int32, (group, 8, part), 1)
+
+    def unfold(ref):
+        def one(g, carry):
+            at = pl.ds(g * group, group)
+            new = jnp.zeros((group, 8, part), f32)
+            for c in range(last):
+                tail = ref[at, keep:cap, cols(c)].astype(f32)
+                new = jnp.where(spare == c, tail[:, 6:7], new)
+                new = jnp.where(spare == last + c, tail[:, 7:8], new)
+            ref[at, keep:cap, cols(last)] = new.astype(bf16)
+            return carry
+
+        lax.fori_loop(0, GROUPS, one, 0)
+
     for c in range(chunks):
-        send_all(out_ref, arrived, c, c)
+
+        def gather(g, carry, c=c):
+            row = g * rows + lax.broadcasted_iota(jnp.int32, (rows, rows_dev), 0)
+
+            def named(target):
+                return sum((target == slot).astype(f32) for slot in slots).astype(bf16)
+
+            y = jnp.dot(named(row), normed[:, cols(c)], preferred_element_type=f32)
+            if fold and c < last:
+                at = lax.rem(row, cap)
+                aim = jnp.where(at == tight, row - 6 + c, jnp.where(at == tight + 1, row - 4 + c, -1))
+                y = y + jnp.dot(named(aim), normed[:, cols(last)], preferred_element_type=f32)
+            sent[pl.ds(g * group, group), :, cols(c)] = y.astype(bf16).reshape(group, cap, part)
+            return carry
+
+        lax.fori_loop(0, GROUPS, gather, 0)
+        send_all(sent, arrived, c, c)
+
+    def weights(g, carry):
+        at = pl.ds(pl.multiple_of(g * WEIGH_COLS, WEIGH_COLS), WEIGH_COLS)
+        row = g * WEIGH_COLS + lax.broadcasted_iota(jnp.int32, (WEIGH_COLS, rows_dev), 0)
+        mix = sum(
+            jnp.where(row == slot, weight_ref[pl.ds(k, 1), :], 0.0) for k, slot in enumerate(slots)
+        ).T
+        for i in range(weigh.shape[0]):
+            piece = mix.astype(bf16)
+            weigh[i, :, at] = piece
+            mix = mix - piece.astype(f32)
+        return carry
+
+    lax.fori_loop(0, n * cap // WEIGH_COLS, weights, 0)
     for load in loads[:2]:
         load.wait()
-    group = n // GROUPS
-    rows = group * cap
 
     for c in range(chunks):
-        wait_all(out_ref, arrived, c, c)
+        wait_all(sent, arrived, c, c)
 
         def gate_up(g, carry, c=c):
             x = arrived[pl.ds(g * group, group), :, cols(c)].reshape(rows, part)
             at = pl.ds(pl.multiple_of(g * rows, rows), rows)
-            gate = jnp.dot(x, wg[cols(c), :], preferred_element_type=jnp.float32)
-            up = jnp.dot(x, wu[cols(c), :], preferred_element_type=jnp.float32)
+            gate = jnp.dot(x, wg[cols(c), :], preferred_element_type=f32)
+            up = jnp.dot(x, wu[cols(c), :], preferred_element_type=f32)
             if c > 0:
                 gate, up = gate + gate_acc[at, :], up + up_acc[at, :]
-            if c < chunks - 1:
+            if c < last:
                 gate_acc[at, :] = gate
                 up_acc[at, :] = up
             else:
-                hidden[at, :] = (jax.nn.silu(gate) * up).astype(jnp.bfloat16)
+                hidden[at, :] = (jax.nn.silu(gate) * up).astype(bf16)
             return carry
 
         lax.fori_loop(0, GROUPS, gate_up, 0)
+        if fold and c == last - 1:
+            unfold(arrived)
     loads[2].wait()
-    for c in range(chunks):
+    order = (last, *range(last))
+    for c in order:
 
         def down(g, carry, c=c):
             at = pl.ds(pl.multiple_of(g * rows, rows), rows)
-            y = jnp.dot(hidden[at, :], wd[:, cols(c)], preferred_element_type=jnp.float32)
-            made[pl.ds(g * group, group), :, cols(c)] = y.astype(jnp.bfloat16).reshape(group, cap, part)
+            some = pl.ds(g * group, group)
+            y = jnp.dot(hidden[at, :], wd[:, cols(c)], preferred_element_type=f32)
+            made[some, :, cols(c)] = y.astype(bf16).reshape(group, cap, part)
+            if fold and c < last:
+                tail = made[some, keep:cap, cols(c)].astype(f32)
+                other = made[some, keep:cap, cols(last)].astype(f32)
+                tail = jnp.where(spare == 6, other[:, c : c + 1], tail)
+                tail = jnp.where(spare == 7, other[:, last + c : last + c + 1], tail)
+                made[some, keep:cap, cols(c)] = tail.astype(bf16)
             return carry
 
         lax.fori_loop(0, GROUPS, down, 0)
         send_all(made, returned, c, chunks + c)
-    total = jnp.zeros((o_ref.shape[0], 1), jnp.float32)
-    for c in range(chunks):
-        wait_all(made, returned, c, chunks + c)
+    total = jnp.zeros((rows_dev, 1), f32)
+
+    def combine(c, total):
         back = returned[:, :, cols(c)].reshape(n * cap, part)
         mixed = sum(
-            jnp.dot(weigh_ref[i], back, preferred_element_type=jnp.float32)
-            for i in range(weigh_ref.shape[0])
+            jnp.dot(weigh[i], back, preferred_element_type=f32) for i in range(weigh.shape[0])
         )
         comb[:, cols(c)] = mixed
-        total = total + jnp.sum(mixed * mixed, axis=1, keepdims=True)
+        return total + jnp.sum(mixed * mixed, axis=1, keepdims=True)
+
+    for c in order:
+        wait_all(made, returned, c, chunks + c)
+        if not (fold and c == last):
+            total = combine(c, total)
+    if fold:
+        unfold(returned)
+        total = combine(last, total)
     scale = lax.rsqrt(total / width + NORM_EPS)
     for c in range(chunks):
         o_ref[:, cols(c)] = (
-            stream_ref[:, cols(c)].astype(jnp.float32) + comb[:, cols(c)] * scale * gain_ref[:, cols(c)]
-        ).astype(jnp.bfloat16)
+            stream[:, cols(c)].astype(f32) + comb[:, cols(c)] * scale * gains_ref[pl.ds(2, 1), cols(c)]
+        ).astype(bf16)
     for c in range(chunks):
-        all_copies(out_ref, arrived, c, c).wait_send()
+        all_copies(sent, arrived, c, c).wait_send()
         all_copies(made, returned, c, chunks + c).wait_send()
 
 
-def experts(outgoing, w_gate, w_up, w_down, weigh, stream, gain, n_tp):
-    n, cap, width = outgoing.shape
+def experts(heads, out_weight, residual, gains, ids, weight, w_gate, w_up, w_down, n, n_tp, tight):
+    rows_dev, width = residual.shape
+    cap = (tight + 7) // 8 * 8
     hidden = w_gate.shape[1]
     slots = n * cap
     chunks = CHUNKS
@@ -445,11 +547,12 @@
     hbm = pl.BlockSpec(memory_space=pl.ANY)
     bf16, f32 = jnp.bfloat16, jnp.float32
     return pl.pallas_call(
-        functools.partial(expert_kernel, n_tp=n_tp, chunks=chunks),
-        out_shape=jax.ShapeDtypeStruct(stream.shape, bf16),
-        in_specs=[vmem, hbm, hbm, hbm, vmem, vmem, vmem],
+        functools.partial(expert_kernel, n_tp=n_tp, chunks=chunks, tight=tight),
+        out_shape=jax.ShapeDtypeStruct(residual.shape, bf16),
+        in_specs=[vmem] * 6 + [hbm] * 3,
         out_specs=vmem,
         scratch_shapes=[
+            pltpu.VMEM((n, cap, width), bf16),
             pltpu.VMEM((n, cap, width), bf16),
             pltpu.VMEM((n, cap, width), bf16),
             pltpu.VMEM((n, cap, width), bf16),
@@ -459,17 +562,20 @@
             pltpu.VMEM((slots, hidden), f32),
             pltpu.VMEM((slots, hidden), f32),
             pltpu.VMEM((slots, hidden), bf16),
-            pltpu.VMEM(stream.shape, f32),
+            pltpu.VMEM(residual.shape, f32),
+            pltpu.VMEM(residual.shape, bf16),
+            pltpu.VMEM(residual.shape, bf16),
+            pltpu.VMEM((2, rows_dev, slots), bf16),
             pltpu.SemaphoreType.DMA((3,)),
             pltpu.SemaphoreType.DMA((2 * chunks,)),
             pltpu.SemaphoreType.DMA((2 * chunks,)),
             pltpu.SemaphoreType.DMA((2 * chunks,)),
         ],
         compiler_params=pltpu.CompilerParams(
-            collective_id=1, has_side_effects=True, vmem_limit_bytes=60 * 2**20
+            collective_id=1, has_side_effects=True, vmem_limit_bytes=56 * 2**20
         ),
         name="experts",
-    )(outgoing, w_gate, w_up, w_down, weigh, stream, gain)
+    )(heads, out_weight, residual, gains, ids, weight, w_gate, w_up, w_down)
 
 
 def local(
@@ -515,33 +621,12 @@
     side_k = side_lanes([ones_k] * 3 + bf16_parts(-gate))
     side_k = side_k.reshape(n_sp, tok_dev, 2 * HEAD_DIM)
     head_rows = attend(kv, q, side_q, side_k, n_tp)
-    projected = jnp.dot(head_rows, out_weight, preferred_element_type=jnp.float32)
-    stream = (residual.astype(jnp.float32) + rms_scale(projected, gain_mix)).astype(jnp.bfloat16)
-    stream_wide = lax.optimization_barrier(stream).astype(jnp.float32)
-    normed = rms_scale(stream_wide, gain_pre).astype(jnp.bfloat16)
     top_count = route_ids.shape[1]
     experts_all = n_sp * n_tp
-    capacity = max(2, (4 * rows_dev * top_count + 3 * experts_all - 1) // (3 * experts_all))
-    capacity = (capacity + 7) // 8 * 8
-    flat_ids = route_ids.reshape(-1)
-    item = lax.iota(jnp.int32, rows_dev * top_count)
-    earlier = (item[None, :] < item[:, None]) & (flat_ids[None, :] == flat_ids[:, None])
-    slot_index = flat_ids * capacity + jnp.sum(earlier.astype(jnp.int32), axis=1)
-    slot_index = slot_index.reshape(rows_dev, top_count)
-    slots_all = experts_all * capacity
-    slot = lax.iota(jnp.int32, slots_all)
-    place = sum((slot_index[:, k, None] == slot).astype(jnp.bfloat16) for k in range(top_count))
-    outgoing = lax.dot_general(
-        place, normed, (((0,), (0,)), ((), ())), preferred_element_type=jnp.float32
-    ).astype(jnp.bfloat16)
-    outgoing = outgoing.reshape(experts_all, capacity, -1)
-    weigh = sum(
-        jnp.where(slot_index[:, k, None] == slot, route_weight[:, k, None], 0.0)
-        for k in range(top_count)
-    )
-    weigh = jnp.stack(bf16_parts(weigh))
+    tight = max(2, (4 * rows_dev * top_count + 3 * experts_all - 1) // (3 * experts_all))
     return experts(
-        outgoing, w_gate[0], w_up[0], w_down[0], weigh, stream, gain_post[None, :], n_tp
+        head_rows, out_weight, residual, jnp.stack((gain_mix, gain_pre, gain_post)),
+        route_ids.T, route_weight.T, w_gate[0], w_up[0], w_down[0], experts_all, n_tp, tight,
     )
 
 

time: 249 us -> 229 us (0.920)
  Pallas kernels: 228 us -> 219 us
  matrix products: 9.14 us -> 3.78 us
    pallas_call x1, Pallas kernels: 152 us -> 142 us  [experts(): pl.pallas_call(functools.partial(expert_kernel, n_tp=n_tp, chunks=chunks,...]
    dot_general x2 -> x0, matrix products: 5.36 us -> none  [the longest x1 2.89 us: local(): lax.dot_general(place, normed, (((0,), (0,)), ((), ())), preferred_elemen...]
where the time goes in v3:
time: 229 us
  Pallas kernels  219 us (96%)
  local copies, waits for them, and re-layouts  4.52 us (2%)
  matrix products  3.78 us (2%)
    pallas_call x1, Pallas kernels, experts(): pl.pallas_call(functools.partial(expert_kernel, n_tp=n_tp, chunks=chunks,...  142 us
    pallas_call x1, Pallas kernels, attend(): pl.pallas_call(functools.partial(attend_kernel, n_tp=n_tp, local_heads=lo...  76.2 us

profile of v3, /device:TPU:27, one launch (start us, length us, event | category | flops | bytes accessed | tf_op | source)
XLA Modules:
  0.0 228.9 jit_solution(15044347966525233548)
XLA Ops:
  0.0 0.0 copy-start.1
  0.0 0.0 copy-start.2
  0.0 0.0 copy-start.3
  0.0 1.1 fusion.1
  1.2 0.2 stack.33
  1.5 2.3 convolution_convert_fusion
  3.8 0.1 stack.31
  4.0 1.5 convolution_convert_fusion.1.side_q_ref
  5.5 0.0 copy-done.1
  5.5 0.0 copy-done.2
  5.5 0.0 copy-done.3
  5.5 0.5 pack.1
  6.0 0.0 copy-start
  6.0 1.0 copy-done
  6.9 0.0 copy-start.4
  6.9 0.8 copy-done.4
  7.7 0.0 copy-start.5
  7.7 76.2 %attend.1.heads_ref = bf16[256,1024]{1,0:T(8,128)(2,1)} custom-call(bf16[4,1024,128]{2,1,0:T(8,128)(2,1)} %copy-done, bf16[8,256,128]{2,1,0:T(8,128)(2,1)} %copy-done.4, bf16[4096,128]{1,0:T(8,128)(2,1)} %convolution_convert_fusion.1.side_q_ref, bf16[8,1024,128]{2,1,0:T(8,128)(2,1)} %bitcast.19), custom_call_target="tpu_custom_call" | custom-call | tf_op jit(solution)/shard_map/attend/pallas_call | solution.py:288
  84.0 0.0 copy-done.5
  84.0 0.0 copy-done.6
  84.0 0.0 copy-done.7
  84.0 0.6 pad_maximum_fusion.gains_ref
  84.7 141.9 %experts.1 = bf16[256,2048]{1,0:T(8,128)(2,1)} custom-call(bf16[256,1024]{1,0:T(8,128)(2,1)} %attend.1.heads_ref, bf16[1024,2048]{1,0:T(8,128)(2,1)} %ow_ref.1, bf16[256,2048]{1,0:T(8,128)(2,1)} %res_ref.1, f32[3,2048]{1,0:T(4,128)} %pad_maximum_fusion.gains_ref, s32[2,256]{1,0:T(2,128)} %bitcast.27, f32[2,256]{1,0:T(2,128)} %bitcast.28, ...), custom_call_target="tpu_custom_call" | custom-call | tf_op jit(solution)/shard_map/experts/pallas_call | solution.py:549
  226.6 2.3 %copy.16 = bf16[256,2048]{1,0:T(8,128)(2,1)} copy(bf16[256,2048]{1,0:T(8,128)(2,1)} %experts.1) | data formatting | bytes 2097152
  (9 shorter events, 0.2 us)
Async XLA Ops:
  0.0 5.5 %copy-start.1 = (bf16[1024,256]{1,0:T(8,128)(2,1)S(1)}, bf16[1024,256]{1,0:T(8,128)(2,1)}, u32[]{:S(2)}) copy-start(bf16[1024,256]{1,0:T(8,128)(2,1)} %q_ref.1) | copy-start | bytes 1572868
  0.0 5.5 %copy-start.2 = (bf16[1024,256]{1,0:T(8,128)(2,1)S(1)}, bf16[1024,256]{1,0:T(8,128)(2,1)}, u32[]{:S(2)}) copy-start(bf16[1024,256]{1,0:T(8,128)(2,1)} %k_ref.1) | copy-start | bytes 1572868
  0.0 5.5 %copy-start.3 = (bf16[1024,256]{1,0:T(8,128)(2,1)S(1)}, bf16[1024,256]{1,0:T(8,128)(2,1)}, u32[]{:S(2)}) copy-start(bf16[1024,256]{1,0:T(8,128)(2,1)} %v_ref.1) | copy-start | bytes 1572868
  6.0 1.0 copy-start
  6.9 0.8 copy-start.4
  7.7 76.2 %copy-start.5 = (f32[2048]{0:T(1024)S(1)}, f32[2048]{0:T(1024)}, u32[]{:S(2)}) copy-start(f32[2048]{0:T(1024)} %param.22) | copy-start | bytes 24580
  7.7 76.2 %copy-start.6 = (f32[2048]{0:T(1024)S(1)}, f32[2048]{0:T(1024)}, u32[]{:S(2)}) copy-start(f32[2048]{0:T(1024)} %param.21) | copy-start | bytes 24580
  7.7 76.3 %copy-start.7 = (f32[2048]{0:T(1024)S(1)}, f32[2048]{0:T(1024)}, u32[]{:S(2)}) copy-start(f32[2048]{0:T(1024)} %param.20) | copy-start | bytes 24580

commit v4 on v3

--- a/solution.py
+++ b/solution.py
@@ -14,61 +14,21 @@
 MESH = pl.DeviceIdType.MESH
 CHUNKS = 4
 GROUPS = 4
-KEY_PARTS = 1
+EXP2_SCALE = math.log2(math.e)
 WEIGH_COLS = 256
 
 
-def bf16_parts(values):
-    parts = []
-    for _ in range(3):
-        part = lax.reduce_precision(values, 8, 7)
-        parts.append(part.astype(jnp.bfloat16))
-        values = values - part
-    return parts
-
-
-def pack_kernel(q_ref, k_ref, v_ref, kv_out, q_out, *, shares, n_tp):
-    tok_dev, width = q_ref.shape
-    rows_dev = tok_dev // n_tp
-    sub = rows_dev // shares
-    for h in range(width // HEAD_DIM):
-        cols = pl.ds(h * HEAD_DIM, HEAD_DIM)
-        kv_out[h] = jnp.concatenate((k_ref[:, cols], v_ref[:, cols]), axis=1)
-        for r in range(shares):
-            for t in range(n_tp // 2):
-                low, high = (
-                    q_ref[pl.ds((t + step) * rows_dev + r * sub, sub), cols]
-                    for step in (0, n_tp // 2)
-                )
-                q_out[h * shares + r, pl.ds(t * sub, sub)] = jnp.concatenate((low, high), axis=1)
-
-
-def pack(queries, key_rows, value_rows, shares, n_tp):
-    tok_dev, width = queries.shape
-    heads = width // HEAD_DIM
-    shapes = [
-        (heads, tok_dev, 2 * HEAD_DIM),
-        (heads * shares, tok_dev // shares // 2, 2 * HEAD_DIM),
-    ]
-    return pl.pallas_call(
-        functools.partial(pack_kernel, shares=shares, n_tp=n_tp),
-        out_shape=[jax.ShapeDtypeStruct(shape, jnp.bfloat16) for shape in shapes],
-        in_specs=[pl.BlockSpec(memory_space=pltpu.VMEM)] * 3,
-        out_specs=[pl.BlockSpec(memory_space=pltpu.VMEM)] * 2,
-        compiler_params=pltpu.CompilerParams(vmem_limit_bytes=32 * 2**20),
-        name="pack",
-    )(queries, key_rows, value_rows)
-
-
 def attend_kernel(
-    kv_ref, q_ref, side_q_ref, side_k_ref, o_ref,
-    kv_all, q_all, k_aug, v_aug, q_aug, peak_ref, acc_ref, out_ref, heads_ref,
-    own_sem, q_sem, kv_sem, head_sem, send_sem, *, n_tp, local_heads,
+    q_hbm, k_hbm, v_hbm, gate_ref, o_ref,
+    q_in, k_in, v_in, kv_ref, q_ref,
+    kv_all, q_all, k_aug, v_turned, q_aug, side_ref, peak_ref, acc_ref, scores_a, scores_b, out_ref, heads_ref,
+    in_sem, own_sem, q_sem, kv_sem, head_sem, send_sem, *, n_tp, local_heads,
 ):
     groups = local_heads
     n_sp = q_ref.shape[0]
     shares = n_sp // groups
     tok_dev = kv_ref.shape[1]
+    f32, bf16 = jnp.float32, jnp.bfloat16
     chunk = 2 * q_ref.shape[1]
     sub = chunk // n_tp
     rows_dev = sub * shares
@@ -86,6 +46,12 @@
     def block_at(i):
         return plane(i // shares) * shares + lax.rem(rank + lax.rem(i, shares), shares)
 
+    loads = [
+        pltpu.make_async_copy(src, dst, in_sem.at[i])
+        for i, (src, dst) in enumerate(((q_hbm, q_in), (k_hbm, k_in), (v_hbm, v_in)))
+    ]
+    for load in loads:
+        load.start()
     barrier = pltpu.get_barrier_semaphore()
 
     def greet(o, carry):
@@ -95,10 +61,20 @@
         return carry
 
     lax.fori_loop(1, n, greet, 0)
-    own_kv = pltpu.make_async_copy(kv_ref.at[group], kv_all.at[sp], own_sem.at[0])
-    own_q = pltpu.make_async_copy(q_ref.at[sp], q_all.at[sp], own_sem.at[1])
-    own_kv.start()
-    own_q.start()
+    for load in loads:
+        load.wait()
+    for h in range(groups):
+        head = pl.ds(h * HEAD_DIM, HEAD_DIM)
+        kv_ref[h] = jnp.concatenate((k_in[:, head], v_in[:, head]), axis=1)
+        for r in range(shares):
+            for t in range(n_tp // 2):
+                low, high = (
+                    q_in[pl.ds((t + half) * rows_dev + r * sub, sub), head]
+                    for half in (0, n_tp // 2)
+                )
+                q_ref[h * shares + r, pl.ds(t * sub, sub)] = jnp.concatenate((low, high), axis=1)
+    kv_all[sp] = kv_ref[group]
+    q_all[sp] = q_ref[sp]
     pl.semaphore_wait(barrier, n - 1)
 
     def kv_copy(src, block, dest, slot):
@@ -125,42 +101,89 @@
             if s and k == 0:
                 kv_copy(kv_ref.at[plane(s)], sp, dest, 2).start()
 
-    row = lax.broadcasted_iota(jnp.int32, (chunk, 1), 0)
-    pos = row // sub * rows_dev + rank * sub + lax.rem(row, sub)
+    slot = lax.broadcasted_iota(jnp.int32, (8, tok_dev), 0)
+    place = lax.broadcasted_iota(jnp.int32, (8, lanes), 1) - HEAD_DIM
+    place = (place == lax.broadcasted_iota(jnp.int32, (8, lanes), 0)).astype(f32).astype(bf16)
+
+    def spread(rows):
+        return lax.dot_general(
+            rows.astype(bf16), place, (((0,), (0,)), ((), ())), preferred_element_type=f32
+        )
 
     def build(block):
+        at = pl.ds(pl.multiple_of(block * tok_dev, tok_dev), tok_dev)
+        gate = gate_ref[pl.ds(group, 1), at] * EXP2_SCALE
+        for_k = (slot < 3).astype(f32)
+        for_q = ((slot >= 3) & (slot < 6)).astype(f32)
+        for i in range(3):
+            piece = gate.astype(bf16).astype(f32)
+            gate = gate - piece
+            for_k = jnp.where(slot == 3 + i, -piece, for_k)
+            for_q = jnp.where(slot == i, piece, for_q)
+        side_ref[...] = spread(for_q)
         lane = lax.broadcasted_iota(jnp.int32, (tok_dev, lanes), 1)
-        kv = kv_all[block].astype(jnp.float32)
-        side = side_k_ref[block].astype(jnp.float32)
-        k_aug[block] = jnp.where(lane < HEAD_DIM, kv, side).astype(jnp.bfloat16)
-        ones = (lane == 0).astype(jnp.float32)
-        v_aug[block] = jnp.where(lane < HEAD_DIM, ones, kv).astype(jnp.bfloat16)
+        kv = kv_all[block].astype(f32)
+        k_aug[block, :, :lanes] = jnp.where(lane < HEAD_DIM, kv, spread(for_k)).astype(bf16)
+        k_aug[block, :, lanes:] = jnp.where(lane < HEAD_DIM, kv, 0.0).astype(bf16)
+        turned = kv.T
+        v_turned[block, :HEAD_DIM] = turned[HEAD_DIM:].astype(bf16)
+        v_turned[block, HEAD_DIM:] = jnp.ones((16, tok_dev), bf16)
         packed = q_all[block]
         queries = jnp.concatenate((packed[:, :HEAD_DIM], packed[:, HEAD_DIM:]), axis=0)
-        queries = queries * jnp.bfloat16(HEAD_DIM**-0.5)
-        side = side_q_ref[pl.ds(pl.multiple_of(block * chunk, chunk), chunk), HEAD_DIM:]
-        q_aug[block] = jnp.concatenate((queries, side), axis=1)
-        peak_ref[block] = jnp.full((chunk, lanes), MASKED, jnp.float32)
-        acc_ref[block] = jnp.zeros((chunk, lanes), jnp.float32)
-
-    def step(i, j, masked):
-        for part in range(KEY_PARTS):
-            count = tok_dev // KEY_PARTS
-            keys = pl.ds(part * count, count)
-            scores = lax.dot_general(
-                q_aug[i], k_aug[j, keys], (((1,), (1,)), ((), ())),
-                preferred_element_type=jnp.float32,
+        queries = queries.astype(f32) * (HEAD_DIM**-0.5 * EXP2_SCALE)
+        high = queries.astype(bf16)
+        low = (queries - high.astype(f32)).astype(bf16)
+        for t in range(n_tp):
+            rows = pl.ds(t * sub, sub)
+            side = side_ref[pl.ds(pl.multiple_of(t * rows_dev + rank * sub, sub), sub), HEAD_DIM:]
+            q_aug[block, rows, :lanes] = jnp.concatenate(
+                (high[t * sub : (t + 1) * sub], side.astype(bf16)), axis=1
             )
-            if masked:
-                key = part * count + lax.broadcasted_iota(jnp.int32, (1, count), 1)
-                scores = jnp.where(key <= pos, scores, MASKED)
-            before = peak_ref[i]
-            peak = jnp.maximum(before, jnp.max(scores, axis=1, keepdims=True))
-            probs = jnp.exp(scores - jnp.concatenate([peak] * (count // lanes), axis=1)).astype(jnp.bfloat16)
-            peak_ref[i] = peak
-            acc_ref[i] = acc_ref[i] * jnp.exp(before - peak) + jnp.dot(
-                probs, v_aug[j, keys], preferred_element_type=jnp.float32
-            )
+        q_aug[block, :, lanes:] = jnp.concatenate((low, jnp.zeros_like(low)), axis=1)
+        peak_ref[block] = jnp.full((1, chunk), MASKED, f32)
+        acc_ref[block] = jnp.zeros((HEAD_DIM + 16, chunk), f32)
+
+    halves = 2 if chunk >= 512 else 1
+    half_rows = chunk // halves
+    scores = (scores_a, scores_b)[:halves]
+
+    def score(h, i, j):
+        found = lax.dot_general(
+            k_aug[j], q_aug[i, pl.ds(h * half_rows, half_rows)], (((1,), (1,)), ((), ())),
+            preferred_element_type=f32,
+        )
+        scores[h][...] = found
+        return jnp.max(found, axis=0, keepdims=True)
+
+    def weigh(h, top, i, j, masked):
+        rows = pl.ds(h * half_rows, half_rows)
+        count = tok_dev // halves * (h + 1) if masked else tok_dev
+        found = scores[h][:count]
+        if masked:
+            key = lax.broadcasted_iota(jnp.int32, (count, 1), 0)
+            row = lax.broadcasted_iota(jnp.int32, (1, half_rows), 1) + h * half_rows
+            pos = row // sub * rows_dev + rank * sub + lax.rem(row, sub)
+            found = jnp.where(key <= pos, found, MASKED)
+            top = jnp.max(found, axis=0, keepdims=True)
+        before = peak_ref[i, :, rows]
+        peak = jnp.maximum(before, top)
+        probs = jnp.exp2(found - peak).astype(bf16)
+        peak_ref[i, :, rows] = peak
+        acc_ref[i, :, rows] = acc_ref[i, :, rows] * jnp.exp2(before - peak) + jnp.dot(
+            v_turned[j, :, :count], probs, preferred_element_type=f32
+        )
+
+    def step(i, j, i_next, j_next, top, masked):
+        for h in range(halves):
+            ahead = (h + 1, i, j) if h + 1 < halves else (0, i_next, j_next)
+            early = halves > 1 and not (masked and h + 1 == halves)
+            if early:
+                found = score(*ahead)
+            weigh(h, top, i, j, masked)
+            if not early and not masked:
+                found = score(*ahead)
+            top = found if early or not masked else top
+        return top
 
     def head_copy(block, t):
         slot = block * n_tp + t
@@ -170,11 +193,11 @@
             device_id=(block, t), device_id_type=MESH,
         )
 
-    own_head = pltpu.make_async_copy(out_ref.at[me], heads_ref.at[me], own_sem.at[2])
+    own_head = pltpu.make_async_copy(out_ref.at[me], heads_ref.at[me], own_sem)
 
     def finish(block):
         acc = acc_ref[block]
-        out = acc[:, HEAD_DIM:] / acc[:, :1]
+        out = (acc[:HEAD_DIM] / acc[HEAD_DIM : HEAD_DIM + 1]).T
         half = sub // 2
         for t in range(n_tp):
             top, low = (out[t * sub + at : t * sub + at + half] for at in (0, half))
@@ -202,11 +225,6 @@
         s, k = i // shares, lax.rem(i, shares)
         turn = k == shares - 1
 
-        @pl.when(i == 0)
-        def _():
-            own_kv.wait()
-            own_q.wait()
-
         @pl.when(i > 0)
         def _():
             q_copy(q_all.at[block], block, block).wait_recv()
@@ -221,18 +239,22 @@
 
         build(block)
 
-        def pair(m, carry):
-            other = block_at(m)
-            step(jnp.maximum(block, other), jnp.minimum(block, other), False)
+        def blocks(m):
+            other = jnp.where(m < i, block_at(jnp.maximum(i - 1 - m, 0)), block)
+            return jnp.maximum(block, other), jnp.minimum(block, other)
+
+        def pair(m, top):
+            other = block_at(i - 1 - m)
+            top = step(*blocks(m), *blocks(m + 1), top, False)
 
             @pl.when(i == n_sp - 1)
             def _():
                 finish(other)
 
-            return carry
-
-        lax.fori_loop(0, i, pair, 0)
-        step(block, block, True)
+            return top
+
+        top = lax.fori_loop(0, i, pair, score(0, *blocks(0)))
+        step(block, block, block, block, top, True)
 
         @pl.when(turn & (s == 0) & (groups > 1))
         def _():
@@ -276,41 +298,51 @@
     sent(out_ref, n - 1, 4)
 
 
-def attend(kv, q, side_q, side_k, n_tp):
-    local_heads, tok_dev, lanes = kv.shape
-    n_sp, half_chunk = q.shape[:2]
-    chunk = 2 * half_chunk
+def attend(queries, key_rows, value_rows, gate, n_sp, n_tp):
+    tok_dev, width = queries.shape
+    local_heads = width // HEAD_DIM
+    lanes = 2 * HEAD_DIM
+    shares = n_sp // local_heads
+    rows_dev = tok_dev // n_tp
+    sub = rows_dev // shares
+    chunk = n_tp * sub
     n = n_sp * n_tp
-    sub = chunk // n_tp
     bf16, f32 = jnp.bfloat16, jnp.float32
     vmem = pl.BlockSpec(memory_space=pltpu.VMEM)
-    rows_dev = tok_dev // n_tp
+    hbm = pl.BlockSpec(memory_space=pl.ANY)
     return pl.pallas_call(
         functools.partial(attend_kernel, n_tp=n_tp, local_heads=local_heads),
-        out_shape=jax.ShapeDtypeStruct((rows_dev, n_tp * local_heads * HEAD_DIM), bf16),
-        in_specs=[vmem] * 4,
+        out_shape=jax.ShapeDtypeStruct((rows_dev, n_tp * width), bf16),
+        in_specs=[hbm] * 3 + [vmem],
         out_specs=vmem,
-        scratch_shapes=[
+        scratch_shapes=[pltpu.VMEM((tok_dev, width), bf16)] * 3
+        + [
+            pltpu.VMEM((local_heads, tok_dev, lanes), bf16),
+            pltpu.VMEM((n_sp, chunk // 2, lanes), bf16),
             pltpu.VMEM((n_sp, tok_dev, lanes), bf16),
-            pltpu.VMEM((n_sp, half_chunk, lanes), bf16),
-            pltpu.VMEM((n_sp, tok_dev, lanes), bf16),
-            pltpu.VMEM((n_sp, tok_dev, lanes), bf16),
-            pltpu.VMEM((n_sp, chunk, lanes), bf16),
-            pltpu.VMEM((n_sp, chunk, lanes), f32),
-            pltpu.VMEM((n_sp, chunk, lanes), f32),
+            pltpu.VMEM((n_sp, chunk // 2, lanes), bf16),
+            pltpu.VMEM((n_sp, tok_dev, 2 * lanes), bf16),
+            pltpu.VMEM((n_sp, HEAD_DIM + 16, tok_dev), bf16),
+            pltpu.VMEM((n_sp, chunk, 2 * lanes), bf16),
+            pltpu.VMEM((tok_dev, lanes), f32),
+            pltpu.VMEM((n_sp, 1, chunk), f32),
+            pltpu.VMEM((n_sp, HEAD_DIM + 16, chunk), f32),
+            pltpu.VMEM((tok_dev, chunk // 2 if chunk >= 512 else chunk), f32),
+            pltpu.VMEM((tok_dev, chunk // 2 if chunk >= 512 else chunk), f32),
             pltpu.VMEM((n, sub // 2, lanes), bf16),
             pltpu.VMEM((n, sub // 2, lanes), bf16),
             pltpu.SemaphoreType.DMA((3,)),
+            pltpu.SemaphoreType.DMA,
             pltpu.SemaphoreType.DMA((n_sp,)),
             pltpu.SemaphoreType.DMA((n_sp,)),
             pltpu.SemaphoreType.DMA,
             pltpu.SemaphoreType.DMA((5,)),
         ],
         compiler_params=pltpu.CompilerParams(
-            collective_id=0, has_side_effects=True, vmem_limit_bytes=56 * 2**20
+            collective_id=0, has_side_effects=True, vmem_limit_bytes=52 * 2**20
         ),
         name="attend",
-    )(kv, q, side_q, side_k)
+    )(queries, key_rows, value_rows, gate)
 
 
 def expert_kernel(
@@ -594,33 +626,9 @@
     w_up,
     w_down,
 ):
-    tok_dev, feature_width = queries.shape
-    local_heads = feature_width // HEAD_DIM
     n_sp, n_tp = lax.axis_size("sp"), lax.axis_size("tp")
-    shares = n_sp // local_heads
     rows_dev = residual.shape[0]
-    sub = rows_dev // shares
-    chunk = n_tp * sub
-    kv, q = pack(queries, key_rows, value_rows, shares, n_tp)
-
-    me = lax.axis_index("sp")
-    gate = lax.dynamic_index_in_dim(cum_gate, me // shares, 0, keepdims=False)
-    gate_q = gate.reshape(n_sp * n_tp, shares, sub)
-    gate_q = lax.dynamic_index_in_dim(gate_q, me % shares, 1, keepdims=False).reshape(-1)
-    ones_q = jnp.ones((n_sp * chunk,), jnp.bfloat16)
-    ones_k = jnp.ones((n_sp * tok_dev,), jnp.bfloat16)
-    lanes = jnp.arange(2 * HEAD_DIM)
-    place_side = (lanes == HEAD_DIM + jnp.arange(6)[:, None]).astype(jnp.bfloat16)
-
-    def side_lanes(parts):
-        return lax.dot_general(
-            jnp.stack(parts), place_side, (((0,), (0,)), ((), ())), preferred_element_type=jnp.float32
-        ).astype(jnp.bfloat16)
-
-    side_q = side_lanes(bf16_parts(gate_q) + [ones_q] * 3)
-    side_k = side_lanes([ones_k] * 3 + bf16_parts(-gate))
-    side_k = side_k.reshape(n_sp, tok_dev, 2 * HEAD_DIM)
-    head_rows = attend(kv, q, side_q, side_k, n_tp)
+    head_rows = attend(queries, key_rows, value_rows, cum_gate, n_sp, n_tp)
     top_count = route_ids.shape[1]
     experts_all = n_sp * n_tp
     tight = max(2, (4 * rows_dev * top_count + 3 * experts_all - 1) // (3 * experts_all))

time: 229 us -> 222 us (0.969)
  Pallas kernels: 219 us -> 214 us
  matrix products: 3.78 us -> 0 us
    dot_general x2 -> x0, matrix products: 3.78 us -> none  [side_lanes(): lax.dot_general(jnp.stack(parts), place_side, (((0,), (0,)), ((), ())), p...]
    pallas_call x1, Pallas kernels: 76.2 us -> 72.7 us  [attend(): pl.pallas_call(functools.partial(attend_kernel, n_tp=n_tp, local_heads=lo...]
    unnamed x17 -> x9, local copies, waits for them, and re-layouts: 4.09 us -> 6.08 us
where the time goes in v4:
time: 222 us
  Pallas kernels  214 us (96%)
  local copies, waits for them, and re-layouts  6.08 us (3%)
    pallas_call x1, Pallas kernels, experts(): pl.pallas_call(functools.partial(expert_kernel, n_tp=n_tp, chunks=chunks,...  142 us
    pallas_call x1, Pallas kernels, attend(): pl.pallas_call(functools.partial(attend_kernel, n_tp=n_tp, local_heads=lo...  72.7 us
    unnamed x9, local copies, waits for them, and re-layouts  6.08 us

profile of v4, /device:TPU:27, one launch (start us, length us, event | category | flops | bytes accessed | tf_op | source)
XLA Modules:
  0.0 221.9 jit_solution(1745094491637921785)
XLA Ops:
  0.0 1.4 pad_maximum_fusion.gains_ref
  1.4 0.0 copy-start.1
  1.4 1.0 copy-done.1
  2.4 0.0 copy-start.2
  2.4 1.0 copy-done.2
  3.4 0.0 copy-start.3
  3.5 0.9 copy-done.3
  4.4 72.7 %attend.1.heads_ref = bf16[256,1024]{1,0:T(8,128)(2,1)S(1)} custom-call(bf16[1024,256]{1,0:T(8,128)(2,1)S(1)} %copy-done.1, bf16[1024,256]{1,0:T(8,128)(2,1)S(1)} %copy-done.2, bf16[1024,256]{1,0:T(8,128)(2,1)} %v_hbm.1, f32[4,8192]{1,0:T(4,128)S(1)} %copy-done.3), custom_call_target="tpu_custom_call" | custom-call | tf_op jit(solution)/shard_map/attend/pallas_call | solution.py:313
  77.0 0.0 copy-start
  77.1 0.8 copy-done
  77.8 141.8 %experts.1 = bf16[256,2048]{1,0:T(8,128)(2,1)} custom-call(bf16[256,1024]{1,0:T(8,128)(2,1)} %copy-done, bf16[1024,2048]{1,0:T(8,128)(2,1)} %ow_ref.1, bf16[256,2048]{1,0:T(8,128)(2,1)} %res_ref.1, f32[3,2048]{1,0:T(4,128)} %pad_maximum_fusion.gains_ref, s32[2,256]{1,0:T(2,128)} %bitcast.14, f32[2,256]{1,0:T(2,128)} %bitcast.15, bf16[2048,512]{1,0:T(8,128)(2,1)} %bitcast.8, ...), custom_call_target="tpu_custom_call" | custom-call | tf_op jit(solution)/shard_map/experts/pallas_call | solution.py:581
  219.6 2.3 %copy.16 = bf16[256,2048]{1,0:T(8,128)(2,1)} copy(bf16[256,2048]{1,0:T(8,128)(2,1)} %experts.1) | data formatting | bytes 2097152
Async XLA Ops:
  1.4 1.0 copy-start.1
  2.4 1.0 copy-start.2
  3.4 0.9 copy-start.3
  77.0 0.8 copy-start

commit v5 on v4

--- a/solution.py
+++ b/solution.py
@@ -16,6 +16,7 @@
 GROUPS = 4
 EXP2_SCALE = math.log2(math.e)
 WEIGH_COLS = 256
+KV_PARTS = 2
 
 
 def attend_kernel(
@@ -43,6 +44,13 @@
         up = jnp.where(s <= groups - 1 - group, group + s, groups - 1 - s)
         return jnp.where(2 * group < groups, down, up)
 
+    def target(s):
+        down = jnp.where(group > 0, groups + group - s, s)
+        down = jnp.where(s <= group, group - s, down)
+        up = jnp.where(group < groups - 1, s - groups + group, groups - 1 - s)
+        up = jnp.where(s <= groups - 1 - group, group + s, up)
+        return jnp.where(2 * group < groups, down, up)
+
     def block_at(i):
         return plane(i // shares) * shares + lax.rem(rank + lax.rem(i, shares), shares)
 
@@ -77,12 +85,21 @@
     q_all[sp] = q_ref[sp]
     pl.semaphore_wait(barrier, n - 1)
 
-    def kv_copy(src, block, dest, slot):
-        return pltpu.make_async_remote_copy(
-            src_ref=src, dst_ref=kv_all.at[block],
-            send_sem=send_sem.at[slot], recv_sem=kv_sem.at[block],
-            device_id=(dest, tp), device_id_type=MESH,
-        )
+    def kv_copies(src, index, block, dest, slot):
+        size = tok_dev // KV_PARTS
+        return [
+            pltpu.make_async_remote_copy(
+                src_ref=src.at[index, pl.ds(part * size, size)],
+                dst_ref=kv_all.at[block, pl.ds(part * size, size)],
+                send_sem=send_sem.at[slot], recv_sem=kv_sem.at[block, part],
+                device_id=(dest, tp), device_id_type=MESH,
+            )
+            for part in range(KV_PARTS)
+        ]
+
+    def kv_send(*where):
+        for copy in kv_copies(*where):
+            copy.start()
 
     def q_copy(src, block, dest):
         return pltpu.make_async_remote_copy(
@@ -93,13 +110,13 @@
 
     for s in range(groups):
         for k in range(shares):
-            dest = block_at(s * shares + k)
+            dest = block_at(k) if s == 0 else target(s) * shares + lax.rem(rank + k, shares)
             if s or k:
                 q_copy(q_ref.at[dest], sp, dest).start()
             if s == 0 and k:
-                kv_copy(kv_ref.at[group], sp, dest, 1).start()
+                kv_send(kv_ref, group, sp, dest, 1)
             if s and k == 0:
-                kv_copy(kv_ref.at[plane(s)], sp, dest, 2).start()
+                kv_send(kv_ref, target(s), sp, dest, 2)
 
     slot = lax.broadcasted_iota(jnp.int32, (8, tok_dev), 0)
     place = lax.broadcasted_iota(jnp.int32, (8, lanes), 1) - HEAD_DIM
@@ -215,15 +232,22 @@
 
     def relay(i):
         block = block_at(i)
-        kv_copy(kv_all.at[block], block, block, 3).wait_recv()
-        for k in range(1, shares):
-            dest = group * shares + lax.rem(rank + k, shares)
-            kv_copy(kv_all.at[block], block, dest, 3).start()
+        for part in range(KV_PARTS):
+            kv_copies(kv_all, block, block, block, 3)[part].wait_recv()
+            for k in range(1, shares):
+                dest = group * shares + lax.rem(rank + k, shares)
+                kv_copies(kv_all, block, block, dest, 3)[part].start()
 
     def one_block(i, carry):
         block = block_at(i)
         s, k = i // shares, lax.rem(i, shares)
-        turn = k == shares - 1
+        turn = (k == shares - 1) & (s < groups - 1)
+        outer = (group == 0) | (group == groups - 1)
+        early = (s > 0) & jnp.where(outer, s < groups - 2, s == groups - 2)
+
+        @pl.when(turn & early)
+        def _():
+            relay(i + 1)
 
         @pl.when(i > 0)
         def _():
@@ -231,11 +255,8 @@
 
         @pl.when(k > 0)
         def _():
-            kv_copy(kv_all.at[block], block, block, 3).wait_recv()
-
-        @pl.when(turn & (s > 0) & (s < groups - 1))
-        def _():
-            relay(i + 1)
+            for copy in kv_copies(kv_all, block, block, block, 3):
+                copy.wait_recv()
 
         build(block)
 
@@ -256,7 +277,7 @@
         top = lax.fori_loop(0, i, pair, score(0, *blocks(0)))
         step(block, block, block, block, top, True)
 
-        @pl.when(turn & (s == 0) & (groups > 1))
+        @pl.when(turn & jnp.logical_not(early))
         def _():
             relay(i + 1)
 
@@ -334,20 +355,20 @@
             pltpu.SemaphoreType.DMA((3,)),
             pltpu.SemaphoreType.DMA,
             pltpu.SemaphoreType.DMA((n_sp,)),
-            pltpu.SemaphoreType.DMA((n_sp,)),
+            pltpu.SemaphoreType.DMA((n_sp, KV_PARTS)),
             pltpu.SemaphoreType.DMA,
             pltpu.SemaphoreType.DMA((5,)),
         ],
         compiler_params=pltpu.CompilerParams(
-            collective_id=0, has_side_effects=True, vmem_limit_bytes=52 * 2**20
+            collective_id=0, has_side_effects=True, vmem_limit_bytes=60 * 2**20
         ),
         name="attend",
     )(queries, key_rows, value_rows, gate)
 
 
 def expert_kernel(
-    heads_ref, ow_ref, res_ref, gains_ref, ids_ref, weight_ref, wg_hbm, wu_hbm, wd_hbm, o_ref,
-    sent, arrived, made, returned, wg, wu, wd, gate_acc, up_acc, hidden, comb, stream, normed, weigh,
+    heads_ref, ow_hbm, res_hbm, mix_ref, pre_ref, post_ref, ids_ref, weight_ref, wg_hbm, wu_hbm, wd_hbm, o_ref,
+    ow_ref, res_ref, sent, arrived, made, returned, wg, wu, wd, gate_acc, up_acc, hidden, comb, stream, normed, weigh,
     w_sem, own_sem, send_sem, recv_sem, *, n_tp, chunks, tight,
 ):
     n, cap, width = sent.shape
@@ -366,11 +387,19 @@
         d = lax.rem(me + o, n)
         return d, (d // n_tp, lax.rem(d, n_tp))
 
+    firsts = [
+        pltpu.make_async_copy(
+            ow_hbm.at[:, pl.ds(c * part, part)], ow_ref.at[:, pl.ds(c * part, part)], w_sem.at[4 + c]
+        )
+        for c in range(chunks)
+    ]
     loads = [
         pltpu.make_async_copy(src, dst, w_sem.at[i])
-        for i, (src, dst) in enumerate(((wg_hbm, wg), (wu_hbm, wu), (wd_hbm, wd)))
+        for i, (src, dst) in enumerate(
+            ((wg_hbm, wg), (wu_hbm, wu), (wd_hbm, wd), (res_hbm, res_ref))
+        )
     ]
-    for load in loads:
+    for load in (*firsts, loads[3], *loads[:3]):
         load.start()
 
     barrier = pltpu.get_barrier_semaphore()
@@ -402,20 +431,22 @@
     heads = heads_ref[...]
     total = jnp.zeros((rows_dev, 1), f32)
     for c in range(chunks):
+        firsts[c].wait()
         proj = jnp.dot(heads, ow_ref[:, cols(c)], preferred_element_type=f32)
         comb[:, cols(c)] = proj
         total = total + jnp.sum(proj * proj, axis=1, keepdims=True)
     scale = lax.rsqrt(total / width + NORM_EPS)
     total = jnp.zeros((rows_dev, 1), f32)
+    loads[3].wait()
     for c in range(chunks):
-        wide = res_ref[:, cols(c)].astype(f32) + comb[:, cols(c)] * scale * gains_ref[pl.ds(0, 1), cols(c)]
+        wide = res_ref[:, cols(c)].astype(f32) + comb[:, cols(c)] * scale * mix_ref[:, cols(c)]
         stream[:, cols(c)] = wide.astype(bf16)
         wide = stream[:, cols(c)].astype(f32)
         total = total + jnp.sum(wide * wide, axis=1, keepdims=True)
     scale = lax.rsqrt(total / width + NORM_EPS)
     for c in range(chunks):
         wide = stream[:, cols(c)].astype(f32)
-        normed[:, cols(c)] = (wide * scale * gains_ref[pl.ds(1, 1), cols(c)]).astype(bf16)
+        normed[:, cols(c)] = (wide * scale * pre_ref[:, cols(c)]).astype(bf16)
     pl.semaphore_wait(barrier, n - 1)
 
     def window(ref, at, c):
@@ -562,14 +593,14 @@
     scale = lax.rsqrt(total / width + NORM_EPS)
     for c in range(chunks):
         o_ref[:, cols(c)] = (
-            stream[:, cols(c)].astype(f32) + comb[:, cols(c)] * scale * gains_ref[pl.ds(2, 1), cols(c)]
+            stream[:, cols(c)].astype(f32) + comb[:, cols(c)] * scale * post_ref[:, cols(c)]
         ).astype(bf16)
     for c in range(chunks):
         all_copies(sent, arrived, c, c).wait_send()
         all_copies(made, returned, c, chunks + c).wait_send()
 
 
-def experts(heads, out_weight, residual, gains, ids, weight, w_gate, w_up, w_down, n, n_tp, tight):
+def experts(heads, out_weight, residual, gain_mix, gain_pre, gain_post, ids, weight, w_gate, w_up, w_down, n, n_tp, tight):
     rows_dev, width = residual.shape
     cap = (tight + 7) // 8 * 8
     hidden = w_gate.shape[1]
@@ -581,9 +612,11 @@
     return pl.pallas_call(
         functools.partial(expert_kernel, n_tp=n_tp, chunks=chunks, tight=tight),
         out_shape=jax.ShapeDtypeStruct(residual.shape, bf16),
-        in_specs=[vmem] * 6 + [hbm] * 3,
+        in_specs=[vmem] + [hbm] * 2 + [vmem] * 5 + [hbm] * 3,
         out_specs=vmem,
         scratch_shapes=[
+            pltpu.VMEM(out_weight.shape, bf16),
+            pltpu.VMEM(residual.shape, bf16),
             pltpu.VMEM((n, cap, width), bf16),
             pltpu.VMEM((n, cap, width), bf16),
             pltpu.VMEM((n, cap, width), bf16),
@@ -598,7 +631,7 @@
             pltpu.VMEM(residual.shape, bf16),
             pltpu.VMEM(residual.shape, bf16),
             pltpu.VMEM((2, rows_dev, slots), bf16),
-            pltpu.SemaphoreType.DMA((3,)),
+            pltpu.SemaphoreType.DMA((4 + chunks,)),
             pltpu.SemaphoreType.DMA((2 * chunks,)),
             pltpu.SemaphoreType.DMA((2 * chunks,)),
             pltpu.SemaphoreType.DMA((2 * chunks,)),
@@ -607,7 +640,7 @@
             collective_id=1, has_side_effects=True, vmem_limit_bytes=56 * 2**20
         ),
         name="experts",
-    )(heads, out_weight, residual, gains, ids, weight, w_gate, w_up, w_down)
+    )(heads, out_weight, residual, gain_mix, gain_pre, gain_post, ids, weight, w_gate, w_up, w_down)
 
 
 def local(
@@ -633,7 +666,7 @@
     experts_all = n_sp * n_tp
     tight = max(2, (4 * rows_dev * top_count + 3 * experts_all - 1) // (3 * experts_all))
     return experts(
-        head_rows, out_weight, residual, jnp.stack((gain_mix, gain_pre, gain_post)),
+        head_rows, out_weight, residual, gain_mix[None], gain_pre[None], gain_post[None],
         route_ids.T, route_weight.T, w_gate[0], w_up[0], w_down[0], experts_all, n_tp, tight,
     )
 

time: 222 us -> 213 us (0.959)
  Pallas kernels: 214 us -> 210 us
  local copies, waits for them, and re-layouts: 6.08 us -> 2.3 us
    unnamed x9 -> x1, local copies, waits for them, and re-layouts: 6.08 us -> 2.3 us
    pallas_call x1, Pallas kernels: 72.7 us -> 69.4 us  [attend(): pl.pallas_call(functools.partial(attend_kernel, n_tp=n_tp, local_heads=lo...]
where the time goes in v5:
time: 213 us
  Pallas kernels  210 us (99%)
  local copies, waits for them, and re-layouts  2.3 us (1%)
    pallas_call x1, Pallas kernels, experts(): pl.pallas_call(functools.partial(expert_kernel, n_tp=n_tp, chunks=chunks,...  141 us
    pallas_call x1, Pallas kernels, attend(): pl.pallas_call(functools.partial(attend_kernel, n_tp=n_tp, local_heads=lo...  69.4 us

profile of v5, /device:TPU:27, one launch (start us, length us, event | category | flops | bytes accessed | tf_op | source)
XLA Modules:
  0.0 212.6 jit_solution(7822661832985979582)
XLA Ops:
  0.0 69.4 %attend.1.heads_ref = bf16[256,1024]{1,0:T(8,128)(2,1)} custom-call(bf16[1024,256]{1,0:T(8,128)(2,1)} %q_hbm.1, bf16[1024,256]{1,0:T(8,128)(2,1)} %k_hbm.1, bf16[1024,256]{1,0:T(8,128)(2,1)} %v_hbm.1, f32[4,8192]{1,0:T(4,128)} %gate_ref.1), custom_call_target="tpu_custom_call" | custom-call | tf_op jit(solution)/shard_map/attend/pallas_call | solution.py:334
  69.4 140.8 %experts.1 = bf16[256,2048]{1,0:T(8,128)(2,1)} custom-call(bf16[256,1024]{1,0:T(8,128)(2,1)} %attend.1.heads_ref, bf16[1024,2048]{1,0:T(8,128)(2,1)} %ow_hbm.1, bf16[256,2048]{1,0:T(8,128)(2,1)} %res_hbm.1, f32[1,2048]{1,0:T(1,128)} %bitcast.11, f32[1,2048]{1,0:T(1,128)} %bitcast.12, f32[1,2048]{1,0:T(1,128)} %bitcast.13, s32[2,256]{1,0:T(2,128)} %bitcast.14, ...), custom_call_target="tpu_custom_call" | custom-call | tf_op jit(solution)/shard_map/experts/pallas_call | solution.py:612
  210.3 2.3 %copy.16 = bf16[256,2048]{1,0:T(8,128)(2,1)} copy(bf16[256,2048]{1,0:T(8,128)(2,1)} %experts.1) | data formatting | bytes 2097152

commit v6 on v5

--- a/solution.py
+++ b/solution.py
@@ -22,9 +22,11 @@
 def attend_kernel(
     q_hbm, k_hbm, v_hbm, gate_ref, o_ref,
     q_in, k_in, v_in, kv_ref, q_ref,
-    kv_all, q_all, k_aug, v_turned, q_aug, side_ref, peak_ref, acc_ref, scores_a, scores_b, out_ref, heads_ref,
-    in_sem, own_sem, q_sem, kv_sem, head_sem, send_sem, *, n_tp, local_heads,
+    kv_all, q_all, k_aug, v_turned, q_aug, side_ref, out_ref, heads_ref,
+    in_sem, own_sem, q_sem, kv_sem, head_sem, send_sem, *halved, n_tp, local_heads,
 ):
+    halves = len(halved) // 3
+    peaks, accs, scores = (halved[i * halves : (i + 1) * halves] for i in range(3))
     groups = local_heads
     n_sp = q_ref.shape[0]
     shares = n_sp // groups
@@ -33,6 +35,7 @@
     chunk = 2 * q_ref.shape[1]
     sub = chunk // n_tp
     rows_dev = sub * shares
+    half_rows = chunk // halves
     lanes = 2 * HEAD_DIM
     n = n_sp * n_tp
     sp, tp = lax.axis_index("sp"), lax.axis_index("tp")
@@ -127,7 +130,7 @@
             rows.astype(bf16), place, (((0,), (0,)), ((), ())), preferred_element_type=f32
         )
 
-    def build(block):
+    def sides(block):
         at = pl.ds(pl.multiple_of(block * tok_dev, tok_dev), tok_dev)
         gate = gate_ref[pl.ds(group, 1), at] * EXP2_SCALE
         for_k = (slot < 3).astype(f32)
@@ -138,9 +141,21 @@
             for_k = jnp.where(slot == 3 + i, -piece, for_k)
             for_q = jnp.where(slot == i, piece, for_q)
         side_ref[...] = spread(for_q)
+        k_aug[block, :, :lanes] = spread(for_k).astype(bf16)
+        for t in range(n_tp):
+            rows = pl.ds(t * sub, sub)
+            side = side_ref[pl.ds(pl.multiple_of(t * rows_dev + rank * sub, sub), sub)]
+            q_aug[block, rows, :lanes] = side.astype(bf16)
+        for h in range(halves):
+            peaks[h][block] = jnp.full((1, half_rows), MASKED, f32)
+            accs[h][block] = jnp.zeros((HEAD_DIM + 16, half_rows), f32)
+
+    def build(block):
         lane = lax.broadcasted_iota(jnp.int32, (tok_dev, lanes), 1)
         kv = kv_all[block].astype(f32)
-        k_aug[block, :, :lanes] = jnp.where(lane < HEAD_DIM, kv, spread(for_k)).astype(bf16)
+        k_aug[block, :, :lanes] = jnp.where(
+            lane < HEAD_DIM, kv, k_aug[block, :, :lanes].astype(f32)
+        ).astype(bf16)
         k_aug[block, :, lanes:] = jnp.where(lane < HEAD_DIM, kv, 0.0).astype(bf16)
         turned = kv.T
         v_turned[block, :HEAD_DIM] = turned[HEAD_DIM:].astype(bf16)
@@ -150,19 +165,8 @@
         queries = queries.astype(f32) * (HEAD_DIM**-0.5 * EXP2_SCALE)
         high = queries.astype(bf16)
         low = (queries - high.astype(f32)).astype(bf16)
-        for t in range(n_tp):
-            rows = pl.ds(t * sub, sub)
-            side = side_ref[pl.ds(pl.multiple_of(t * rows_dev + rank * sub, sub), sub), HEAD_DIM:]
-            q_aug[block, rows, :lanes] = jnp.concatenate(
-                (high[t * sub : (t + 1) * sub], side.astype(bf16)), axis=1
-            )
+        q_aug[block, :, :lanes] = jnp.concatenate((high, q_aug[block, :, HEAD_DIM:lanes]), axis=1)
         q_aug[block, :, lanes:] = jnp.concatenate((low, jnp.zeros_like(low)), axis=1)
-        peak_ref[block] = jnp.full((1, chunk), MASKED, f32)
-        acc_ref[block] = jnp.zeros((HEAD_DIM + 16, chunk), f32)
-
-    halves = 2 if chunk >= 512 else 1
-    half_rows = chunk // halves
-    scores = (scores_a, scores_b)[:halves]
 
     def score(h, i, j):
         found = lax.dot_general(
@@ -173,7 +177,6 @@
         return jnp.max(found, axis=0, keepdims=True)
 
     def weigh(h, top, i, j, masked):
-        rows = pl.ds(h * half_rows, half_rows)
         count = tok_dev // halves * (h + 1) if masked else tok_dev
         found = scores[h][:count]
         if masked:
@@ -182,18 +185,18 @@
             pos = row // sub * rows_dev + rank * sub + lax.rem(row, sub)
             found = jnp.where(key <= pos, found, MASKED)
             top = jnp.max(found, axis=0, keepdims=True)
-        before = peak_ref[i, :, rows]
+        before = peaks[h][i]
         peak = jnp.maximum(before, top)
         probs = jnp.exp2(found - peak).astype(bf16)
-        peak_ref[i, :, rows] = peak
-        acc_ref[i, :, rows] = acc_ref[i, :, rows] * jnp.exp2(before - peak) + jnp.dot(
+        peaks[h][i] = peak
+        accs[h][i] = accs[h][i] * jnp.exp2(before - peak) + jnp.dot(
             v_turned[j, :, :count], probs, preferred_element_type=f32
         )
 
     def step(i, j, i_next, j_next, top, masked):
         for h in range(halves):
             ahead = (h + 1, i, j) if h + 1 < halves else (0, i_next, j_next)
-            early = halves > 1 and not (masked and h + 1 == halves)
+            early = h + 1 < halves
             if early:
                 found = score(*ahead)
             weigh(h, top, i, j, masked)
@@ -213,8 +216,9 @@
     own_head = pltpu.make_async_copy(out_ref.at[me], heads_ref.at[me], own_sem)
 
     def finish(block):
-        acc = acc_ref[block]
-        out = (acc[:HEAD_DIM] / acc[HEAD_DIM : HEAD_DIM + 1]).T
+        parts = [accs[h][block] for h in range(halves)]
+        parts = [(acc[:HEAD_DIM] / acc[HEAD_DIM : HEAD_DIM + 1]).T for acc in parts]
+        out = jnp.concatenate(parts, axis=0)
         half = sub // 2
         for t in range(n_tp):
             top, low = (out[t * sub + at : t * sub + at + half] for at in (0, half))
@@ -283,7 +287,14 @@
 
         return carry
 
-    lax.fori_loop(0, n_sp, one_block, 0)
+    def one_side(i, carry):
+        sides(block_at(i))
+        return carry
+
+    sides(sp)
+    one_block(0, 0)
+    lax.fori_loop(1, n_sp, one_side, 0)
+    lax.fori_loop(1, n_sp, one_block, 0)
     finish(block_at(n_sp - 1))
     own_head.wait()
 
@@ -328,6 +339,8 @@
     sub = rows_dev // shares
     chunk = n_tp * sub
     n = n_sp * n_tp
+    halves = 2 if chunk >= 512 else 1
+    half_rows = chunk // halves
     bf16, f32 = jnp.bfloat16, jnp.float32
     vmem = pl.BlockSpec(memory_space=pltpu.VMEM)
     hbm = pl.BlockSpec(memory_space=pl.ANY)
@@ -346,10 +359,6 @@
             pltpu.VMEM((n_sp, HEAD_DIM + 16, tok_dev), bf16),
             pltpu.VMEM((n_sp, chunk, 2 * lanes), bf16),
             pltpu.VMEM((tok_dev, lanes), f32),
-            pltpu.VMEM((n_sp, 1, chunk), f32),
-            pltpu.VMEM((n_sp, HEAD_DIM + 16, chunk), f32),
-            pltpu.VMEM((tok_dev, chunk // 2 if chunk >= 512 else chunk), f32),
-            pltpu.VMEM((tok_dev, chunk // 2 if chunk >= 512 else chunk), f32),
             pltpu.VMEM((n, sub // 2, lanes), bf16),
             pltpu.VMEM((n, sub // 2, lanes), bf16),
             pltpu.SemaphoreType.DMA((3,)),
@@ -358,7 +367,10 @@
             pltpu.SemaphoreType.DMA((n_sp, KV_PARTS)),
             pltpu.SemaphoreType.DMA,
             pltpu.SemaphoreType.DMA((5,)),
-        ],
+        ]
+        + [pltpu.VMEM((n_sp, 1, half_rows), f32)] * halves
+        + [pltpu.VMEM((n_sp, HEAD_DIM + 16, half_rows), f32)] * halves
+        + [pltpu.VMEM((tok_dev, half_rows), f32)] * halves,
         compiler_params=pltpu.CompilerParams(
             collective_id=0, has_side_effects=True, vmem_limit_bytes=60 * 2**20
         ),

time: 213 us -> 210 us (0.986)
    pallas_call x1, Pallas kernels: 69.4 us -> 67 us  [attend(): pl.pallas_call(functools.partial(attend_kernel, n_tp=n_tp, local_heads=lo...]
where the time goes in v6:
time: 210 us
  Pallas kernels  208 us (99%)
  local copies, waits for them, and re-layouts  2.3 us (1%)
    pallas_call x1, Pallas kernels, experts(): pl.pallas_call(functools.partial(expert_kernel, n_tp=n_tp, chunks=chunks,...  141 us
    pallas_call x1, Pallas kernels, attend(): pl.pallas_call(functools.partial(attend_kernel, n_tp=n_tp, local_heads=lo...  67 us

profile of v6, /device:TPU:27, one launch (start us, length us, event | category | flops | bytes accessed | tf_op | source)
XLA Modules:
  0.0 210.0 jit_solution(9248589015195416416)
XLA Ops:
  0.0 67.0 %attend.1.heads_ref = bf16[256,1024]{1,0:T(8,128)(2,1)} custom-call(bf16[1024,256]{1,0:T(8,128)(2,1)} %q_hbm.1, bf16[1024,256]{1,0:T(8,128)(2,1)} %k_hbm.1, bf16[1024,256]{1,0:T(8,128)(2,1)} %v_hbm.1, f32[4,8192]{1,0:T(4,128)} %gate_ref.1), custom_call_target="tpu_custom_call" | custom-call | tf_op jit(solution)/shard_map/attend/pallas_call | solution.py:347
  67.0 140.7 %experts.1 = bf16[256,2048]{1,0:T(8,128)(2,1)} custom-call(bf16[256,1024]{1,0:T(8,128)(2,1)} %attend.1.heads_ref, bf16[1024,2048]{1,0:T(8,128)(2,1)} %ow_hbm.1, bf16[256,2048]{1,0:T(8,128)(2,1)} %res_hbm.1, f32[1,2048]{1,0:T(1,128)} %bitcast.11, f32[1,2048]{1,0:T(1,128)} %bitcast.12, f32[1,2048]{1,0:T(1,128)} %bitcast.13, s32[2,256]{1,0:T(2,128)} %bitcast.14, ...), custom_call_target="tpu_custom_call" | custom-call | tf_op jit(solution)/shard_map/experts/pallas_call | solution.py:624
  207.7 2.3 %copy.16 = bf16[256,2048]{1,0:T(8,128)(2,1)} copy(bf16[256,2048]{1,0:T(8,128)(2,1)} %experts.1) | data formatting | bytes 2097152

commit v7 on v6

--- a/solution.py
+++ b/solution.py
@@ -16,7 +16,7 @@
 GROUPS = 4
 EXP2_SCALE = math.log2(math.e)
 WEIGH_COLS = 256
-KV_PARTS = 2
+KV_PARTS = 4
 
 
 def attend_kernel(

time: 210 us -> 210 us (level)
  no operation moved by 1% of the time
where the time goes in v7:
time: 210 us; the launch traced here: 209 us
  Pallas kernels  207 us (99%)
  local copies, waits for them, and re-layouts  2.3 us (1%)
    pallas_call x1, Pallas kernels, experts(): pl.pallas_call(functools.partial(expert_kernel, n_tp=n_tp, chunks=chunks,...  141 us
    pallas_call x1, Pallas kernels, attend(): pl.pallas_call(functools.partial(attend_kernel, n_tp=n_tp, local_heads=lo...  66.5 us

profile of v7, /device:TPU:27, one launch (start us, length us, event | category | flops | bytes accessed | tf_op | source)
XLA Modules:
  0.0 209.4 jit_solution(11848422118569839506)
XLA Ops:
  0.0 66.5 %attend.1.heads_ref = bf16[256,1024]{1,0:T(8,128)(2,1)} custom-call(bf16[1024,256]{1,0:T(8,128)(2,1)} %q_hbm.1, bf16[1024,256]{1,0:T(8,128)(2,1)} %k_hbm.1, bf16[1024,256]{1,0:T(8,128)(2,1)} %v_hbm.1, f32[4,8192]{1,0:T(4,128)} %gate_ref.1), custom_call_target="tpu_custom_call" | custom-call | tf_op jit(solution)/shard_map/attend/pallas_call | solution.py:347
  66.5 140.6 %experts.1 = bf16[256,2048]{1,0:T(8,128)(2,1)} custom-call(bf16[256,1024]{1,0:T(8,128)(2,1)} %attend.1.heads_ref, bf16[1024,2048]{1,0:T(8,128)(2,1)} %ow_hbm.1, bf16[256,2048]{1,0:T(8,128)(2,1)} %res_hbm.1, f32[1,2048]{1,0:T(1,128)} %bitcast.11, f32[1,2048]{1,0:T(1,128)} %bitcast.12, f32[1,2048]{1,0:T(1,128)} %bitcast.13, s32[2,256]{1,0:T(2,128)} %bitcast.14, ...), custom_call_target="tpu_custom_call" | custom-call | tf_op jit(solution)/shard_map/experts/pallas_call | solution.py:624
  207.1 2.3 %copy.16 = bf16[256,2048]{1,0:T(8,128)(2,1)} copy(bf16[256,2048]{1,0:T(8,128)(2,1)} %experts.1) | data formatting | bytes 2097152
